TPU v7x, 128 devices: a whole 4x4x4 slice. The times are simulated.
128 devices in a mesh: sp: 16 (over z, x), fs: 4 (over y), tp: 2 (over core).
Axes of the slice: x: 4, y: 4, z: 4, core: 2. Of those that a mesh axis runs over, the one named last changes fastest.
Arguments:
- tokens: bfloat16 [4, 8192, 2048], P('fs', 'sp', 'tp'), may hold values from -6 to 6
- norm_gain: float32 [2048], replicated, may hold values from 0.1 to 1.9
- w_pool_in: bfloat16 [2048, 512], P('fs', 'tp'), may hold values from -0.125 to 0.125
- w_query: bfloat16 [2048, 1024], P('fs', 'tp'), may hold values from -0.125 to 0.125
- w_key: bfloat16 [2048, 1024], P('fs', 'tp'), may hold values from -0.125 to 0.125
- w_value: bfloat16 [2048, 1024], P('fs', 'tp'), may hold values from -0.125 to 0.125
- query_gain: float32 [64], replicated, may hold values from 1.5 to 2.5
- key_gain: float32 [64], replicated, may hold values from 1.5 to 2.5
- stick_offset: float32 [16], P('tp'), as said below
- pool_mix: bfloat16 [4, 128, 128], P('tp'), may hold values from -0.5 to 0.5
- pool_scale: float32 [512], P('tp'), may hold values from 0.2 to 4, as said below
- pool_gain: bfloat16 [512], P('tp'), may hold values from 0.099609375 to 1.8984375
- attn_gain: bfloat16 [1024], P('tp'), may hold values from 0.099609375 to 1.8984375
- w_out_pool: bfloat16 [512, 2048], P('tp', 'fs'), may hold values from -0.15625 to 0.15625
- w_out_attn: bfloat16 [1024, 2048], P('tp', 'fs'), may hold values from -0.15625 to 0.15625
Outputs:
- mixed: bfloat16 [4, 8192, 2048], P('fs', ('sp', 'tp'))
Inputs may be any that keep to these rules, and one draw needn't show every extreme that they name: `stick_offset`: per head, negative. `pool_scale`: positive channel scales.
All inputs are finite; a program needn't handle non-finite values.
Results may differ from a plain program's by a relative error of at most 0.013.
Values may be sent and summed in bfloat16 or wider, within the bound.
A program may use at most 192 MiB of HBM per device.

v0:
```python
import math

import jax
import jax.numpy as jnp
from jax import lax
from jax.sharding import PartitionSpec as P

HEADS = 16
HEAD_DIM = 64
POOL = 512
POOL_GROUPS = 4


EPS = 1e-06


def sent_to_all(shard, axis):
    devices = lax.axis_size(axis)
    return lax.all_to_all(
        jnp.broadcast_to(shard[None], (devices, *shard.shape)), axis, 0, 0, tiled=True
    )


def in_order(parts, dim):
    lengths = list(parts.shape[1:])
    lengths[dim] *= parts.shape[0]
    return jnp.moveaxis(parts, 0, dim).reshape(lengths)


def gathered_copies(shard, axis, dim):
    parts = sent_to_all(shard, axis)
    return in_order(parts, dim)


def in_one_piece(arrays, axis, dim, along):
    both = jnp.concatenate(arrays, axis=along)
    whole, at, outs = (lax.all_gather(both, axis, axis=dim, tiled=True), 0, [])
    for a in arrays:
        outs.append(lax.slice_in_dim(whole, at, at + a.shape[along], axis=along))
        at += a.shape[along]
    return tuple(outs)


def shifted_2(value, axis, steps):
    count = lax.axis_size(axis)
    initial, last = (max(0, -steps), min(count, count - steps))
    return lax.ppermute(value, axis, [(source, source + steps) for source in range(initial, last)])


def partner_2(shard, axis, distance):
    return lax.ppermute(shard, axis, [(i, i ^ 1 << distance) for i in range(lax.axis_size(axis))])


def head_norm(projected, gain, head_count):
    split = projected.reshape(projected.shape[0], head_count, HEAD_DIM)
    factor = lax.rsqrt(jnp.mean(split * split, axis=-1, keepdims=True) + EPS)
    return (split * factor * gain).astype(jnp.bfloat16)


def stick_block(query, key_heads, value_heads, offset, carried, row_offset, score_scale):
    scores = (
        jnp.einsum("thd,khd->htk", query, key_heads, preferred_element_type=jnp.float32)
        * score_scale
        + offset[:, None, None]
    )
    keep = jax.nn.log_sigmoid(-scores)
    if row_offset is not None:
        shape = (query.shape[0], key_heads.shape[0])
        earlier = (
            lax.broadcasted_iota(jnp.int32, shape, 1)
            < lax.broadcasted_iota(jnp.int32, shape, 0) + row_offset
        )
        keep = jnp.where(earlier[None], keep, 0.0)
    running = jnp.cumsum(keep, axis=2)
    block_total = running[:, :, -1]
    log_weight = (
        jax.nn.log_sigmoid(scores) + block_total[:, :, None] - running + carried[:, :, None]
    )
    weight = jnp.exp(log_weight)
    if row_offset is not None:
        weight = jnp.where(earlier[None], weight, 0.0)
    weight = weight.astype(jnp.bfloat16)
    block_out = jnp.einsum("htk,khd->thd", weight, value_heads, preferred_element_type=jnp.float32)
    return (block_out, block_total)


def branch_norm(values_in, squares, width, gain):
    values_f = values_in.astype(jnp.float32)
    factor = lax.rsqrt(squares / width + EPS)
    return (values_f * factor[:, None] * gain.astype(jnp.float32)).astype(jnp.bfloat16)


def shards(
    tokens,
    norm_gain,
    w_pool_in,
    w_query,
    w_key,
    w_value,
    query_gain,
    key_gain,
    stick_offset,
    pool_mix,
    pool_scale,
    pool_gain,
    attn_gain,
    w_out_pool,
    w_out_attn,
):
    whole = gathered_copies(tokens, "tp", 2)[0]
    whole_f = whole.astype(jnp.float32)
    normed = (
        whole_f * lax.rsqrt(jnp.mean(whole_f * whole_f, axis=-1, keepdims=True) + EPS) * norm_gain
    ).astype(jnp.bfloat16)
    row_count = normed.shape[0]
    pieces = in_one_piece((w_pool_in, w_query, w_key, w_value), "fs", 0, 1)
    pool_raw, query_raw, key_raw, value_raw = tuple(
        (jnp.dot(normed, piece, preferred_element_type=jnp.float32) for piece in pieces)
    )
    head_count = query_raw.shape[1] // HEAD_DIM
    query = head_norm(query_raw, query_gain, head_count)
    key_heads = head_norm(key_raw, key_gain, head_count)
    value_heads = value_raw.astype(jnp.bfloat16).reshape(row_count, head_count, HEAD_DIM)
    reach = 16
    pool_in = pool_raw.astype(jnp.bfloat16)
    previous = shifted_2(pool_in[row_count - reach :], "sp", 1)
    extended = jnp.concatenate([previous, pool_in], axis=0).astype(jnp.float32)
    pool_cols = pool_in.shape[1]
    group_ch = POOL // POOL_GROUPS
    local_groups = pool_cols // group_ch
    group_ids = (
        lax.axis_index("tp") * local_groups + jnp.arange(pool_cols, dtype=jnp.int32) // group_ch
    )
    window = jnp.left_shift(jnp.int32(2), group_ids)
    summed = jnp.zeros((row_count, pool_cols), jnp.float32)
    for behind in range(reach):
        shifted = extended[reach - behind : reach - behind + row_count]
        summed = summed + jnp.where(behind < window[None, :], shifted, 0.0)
    sp_index = lax.axis_index("sp")
    position = sp_index * row_count + jnp.arange(row_count, dtype=jnp.int32)
    counted = jnp.minimum(position[:, None] + 1, window[None, :]).astype(jnp.float32)
    centered = (summed / counted - extended[reach:]).astype(jnp.bfloat16)
    pooled = jnp.einsum(
        "tgc,gcd->tgd",
        centered.reshape(row_count, local_groups, group_ch),
        pool_mix,
        preferred_element_type=jnp.float32,
    )
    pool_out = (pooled.reshape(row_count, pool_cols) * pool_scale).astype(jnp.bfloat16)
    score_scale = 1.0 / math.sqrt(HEAD_DIM)
    sp_count = lax.axis_size("sp")
    key_value = jnp.stack([key_heads, value_heads])
    everything = lax.all_gather(key_value, "sp", axis=1, tiled=True)
    half = row_count // 2
    bit_count = sp_count.bit_length() - 1

    def run_rows(query_rows, source, row_offset):
        start_carry = jnp.zeros((head_count, query_rows.shape[0]), jnp.float32)
        diagonal = lax.dynamic_slice_in_dim(everything, source * row_count, row_count, 1)
        first_out, first_carry = stick_block(
            query_rows, diagonal[0], diagonal[1], stick_offset, start_carry, row_offset, score_scale
        )

        def turn(turn_index, state):
            acc_out, acc_carry = state
            block = lax.dynamic_slice_in_dim(
                everything, (source - turn_index) * row_count, row_count, 1
            )
            block_out, block_total = stick_block(
                query_rows, block[0], block[1], stick_offset, acc_carry, None, score_scale
            )
            return (acc_out + block_out, acc_carry + block_total)

        result, unused = lax.fori_loop(1, source + 1, turn, (first_out, first_carry))
        return result.reshape(query_rows.shape[0], head_count * HEAD_DIM).astype(jnp.bfloat16)

    guest_query = query[half:]
    for bit in range(bit_count):
        guest_query = partner_2(guest_query, "sp", bit)
    partner = sp_count - 1 - sp_index
    own_rows = run_rows(query[:half], sp_index, 0)
    guest_rows = run_rows(guest_query, partner, half)
    for bit in range(bit_count):
        guest_rows = partner_2(guest_rows, "sp", bit)
    attn_out = jnp.concatenate([own_rows, guest_rows], axis=0)
    w_pool_cols, w_attn_cols = (
        lax.all_gather(w_out_pool, "fs", axis=1, tiled=True),
        lax.all_gather(w_out_attn, "fs", axis=1, tiled=True),
    )
    pool_rows, attn_rows = (
        lax.all_to_all(pool_out, "tp", split_axis=0, concat_axis=1, tiled=True),
        lax.all_to_all(attn_out, "tp", split_axis=0, concat_axis=1, tiled=True),
    )
    w_pool_all, w_attn_all, pool_gain_all, attn_gain_all = (
        lax.all_gather(w_pool_cols, "tp", axis=0, tiled=True),
        lax.all_gather(w_attn_cols, "tp", axis=0, tiled=True),
        lax.all_gather(pool_gain, "tp", axis=0, tiled=True),
        lax.all_gather(attn_gain, "tp", axis=0, tiled=True),
    )
    pool_f = pool_rows.astype(jnp.float32)
    attn_f = attn_rows.astype(jnp.float32)
    pool_normed = branch_norm(pool_rows, jnp.sum(pool_f * pool_f, axis=-1), POOL, pool_gain_all)
    attn_normed = branch_norm(
        attn_rows, jnp.sum(attn_f * attn_f, axis=-1), HEADS * HEAD_DIM, attn_gain_all
    )
    mixed = jnp.dot(pool_normed, w_pool_all, preferred_element_type=jnp.float32) + jnp.dot(
        attn_normed, w_attn_all, preferred_element_type=jnp.float32
    )
    return mixed.astype(jnp.bfloat16)[None]


def solution(mesh):
    in_specs = (
        P("fs", "sp", "tp"),
        P(),
        P("fs", "tp"),
        P("fs", "tp"),
        P("fs", "tp"),
        P("fs", "tp"),
        P(),
        P(),
        P("tp"),
        P("tp", None, None),
        P("tp"),
        P("tp"),
        P("tp"),
        P("tp", "fs"),
        P("tp", "fs"),
    )
    out_specs = P("fs", ("sp", "tp"), None)
    return jax.shard_map(shards, mesh=mesh, in_specs=in_specs, out_specs=out_specs, check_vma=False)
```

profile of v0, /device:TPU:103, one launch (start us, length us, event | category | flops | bytes accessed | tf_op | source)
XLA Modules:
  0.0 760.9 jit_solution(1497514801564157925)
XLA Ops:
  11.9 5.5 all-to-all-start
  27.3 57.7 %all-gather.9.cloned.1.call-done = bf16[2048,1792]{1,0:T(8,128)(2,1)} async-done(((bf16[512,1792]{1,0:T(8,128)(2,1)}), bf16[2048,1792]{1,0:T(8,128)(2,1)}) %all-gather.9.cloned.1.call-update) | async-done | bytes 7340048 | tf_op jit(solution)/shard_map/all_gather | solution.py:37
  101.0 17.3 %all-gather.17.cloned.1.call-done = bf16[512,2048]{1,0:T(8,128)(2,1)} async-done(((bf16[512,512]{1,0:T(8,128)(2,1)}), bf16[512,2048]{1,0:T(8,128)(2,1)}) %all-gather.17.cloned.1.call-update) | async-done | bytes 2097168 | tf_op jit(solution)/shard_map/all_gather | solution.py:188
  134.2 8.0 %all-gather.11.cloned.1.call-done = bf16[256,2048]{1,0:T(8,128)(2,1)} async-done(((bf16[256,512]{1,0:T(8,128)(2,1)}), bf16[256,2048]{1,0:T(8,128)(2,1)}) %all-gather.11.cloned.1.call-update) | async-done | bytes 1048592 | tf_op jit(solution)/shard_map/all_gather | solution.py:187
  146.6 6.6 all-to-all-start.1
  154.5 8.3 %collective-permute-done.3 = bf16[256,8,64]{0,2,1:T(8,128)(2,1)S(1)} collective-permute-done((bf16[256,8,64]{0,2,1:T(8,128)(2,1)S(1)}, bf16[256,8,64]{0,2,1:T(8,128)(2,1)S(1)}, u32[]{:S(2)}, u32[]{:S(2)}) %collective-permute-start.3) | collective-permute-done | bytes 262176 | tf_op jit(solution)/shard_map/ppermute | solution.py:51
  164.9 5.2 collective-permute-done.4
  170.2 98.3 %all-gather.15.cloned.1.call-done = bf16[2,8192,8,64]{1,3,2,0:T(8,128)(2,1)} async-done(((bf16[2,512,8,64]{1,3,2,0:T(8,128)(2,1)}), bf16[2,8192,8,64]{1,3,2,0:T(8,128)(2,1)}) %all-gather.15.cloned.1.call-update) | async-done | bytes 16777232 | tf_op jit(solution)/shard_map/all_gather | solution.py:153
  270.3 10.6 %fusion.63 = (f32[8,256,512]{2,1,0:T(8,128)}, f32[8,256,512]{2,1,0:T(8,128)}, f32[8,256,512]{2,1,0:T(8,128)}) fusion(f32[8]{0:T(128)S(1)} %copy-done.14, pred[256,512]{1,0:T(8,128)(4,1)S(1)} %get-tuple-element.157, f32[8,256,512]{2,1,0:T(8,128)S(1)} %fusion.97, pred[256,512]{1,0:T(8,128)(4,1)S(1)} %get-tuple-element.156, ...), kind=kOutput, calls=%fused_computation.79 | convolution fusion | flops 155189248 | bytes 17826308 | tf_op jit(solution)/shard_map/thd,khd->htk/dot_general | solution.py:62
  280.9 5.7 copy.122
  286.7 5.6 copy.124
  297.3 5.3 copy.125
  304.5 6.4 fusion.88
  311.4 14.4 %collective-permute-start.5 = (bf16[256,512]{0,1:T(8,128)(2,1)S(1)}, bf16[256,512]{0,1:T(8,128)(2,1)S(1)}, u32[]{:S(2)}, u32[]{:S(2)}) collective-permute-start(bf16[256,512]{0,1:T(8,128)(2,1)S(1)} %bitcast.254), channel_id=1, source_target_pairs={{0,8},{8,0},{16,24},{24,16},{32,40},{40,32},{48,56},{56,48},{64,72... | collective-permute-start | bytes 786440 | tf_op jit(solution)/shard_map/ppermute | solution.py:51
  330.5 28.5 %collective-permute-start.6 = (bf16[256,512]{0,1:T(8,128)(2,1)S(1)}, bf16[256,512]{0,1:T(8,128)(2,1)S(1)}, u32[]{:S(2)}, u32[]{:S(2)}) collective-permute-start(bf16[256,512]{0,1:T(8,128)(2,1)S(1)} %collective-permute-done.5), channel_id=1, source_target_pairs={{0,16},{8,24},{16,0},{24,8},{32,48},{40,56},{48,32},{56,40},{64,80... | collective-permute-start | bytes 786440 | tf_op jit(solution)/shard_map/ppermute | solution.py:51
  361.2 5.3 copy.123
  368.3 53.3 %collective-permute-start.7 = (bf16[256,512]{0,1:T(8,128)(2,1)S(1)}, bf16[256,512]{0,1:T(8,128)(2,1)S(1)}, u32[]{:S(2)}, u32[]{:S(2)}) collective-permute-start(bf16[256,512]{0,1:T(8,128)(2,1)S(1)} %collective-permute-done.6), channel_id=1, source_target_pairs={{0,32},{8,40},{16,48},{24,56},{32,0},{40,8},{48,16},{56,24},{64,96... | collective-permute-start | bytes 786440 | tf_op jit(solution)/shard_map/ppermute | solution.py:51
  421.6 6.4 fusion.85
  428.0 110.4 %collective-permute-start.8 = (bf16[256,512]{0,1:T(8,128)(2,1)S(1)}, bf16[256,512]{0,1:T(8,128)(2,1)S(1)}, u32[]{:S(2)}, u32[]{:S(2)}) collective-permute-start(bf16[256,512]{0,1:T(8,128)(2,1)S(1)} %collective-permute-done.7), channel_id=1, source_target_pairs={{0,64},{8,72},{16,80},{24,88},{32,96},{40,104},{48,112},{56,120},{... | collective-permute-start | bytes 786440 | tf_op jit(solution)/shard_map/ppermute | solution.py:51
  538.4 200.4 %while.24 = (s32[]{:T(128)}, f32[256,8,64]{0,2,1:T(8,128)S(1)}, f32[8,256]{1,0:T(8,128)S(1)}, s32[]{:T(128)}, s32[]{:T(128)}, /*index=5*/bf16[2,8192,8,64]{1,3,2...) while((s32[]{:T(128)}, f32[256,8,64]{0,2,1:T(8,128)S(1)}, ...), condition=%wide.region_9.10_spmd, body=%wide.region_6.9_spmd.sunk | while | flops 426934272 | bytes 44548372 | solution.py:174
  547.0 4.7 fusion.179
  560.3 4.7 fusion.179
  573.7 4.7 fusion.179
  587.1 4.7 fusion.179
  600.4 4.7 fusion.179
  613.8 4.7 fusion.179
  627.1 4.7 fusion.179
  640.5 4.7 fusion.179
  667.2 4.7 fusion.179
  694.0 4.7 fusion.179
  720.7 4.7 fusion.179
  739.2 7.0 all_to_all.28
  (270 shorter events, 227.2 us)
Async XLA Ops:
  6.5 137.0 %copy-start = (bf16[2,128,128]{2,1,0:T(8,128)(2,1)S(1)}, bf16[2,128,128]{2,1,0:T(8,128)(2,1)}, u32[]{:S(2)}) copy-start(bf16[2,128,128]{2,1,0:T(8,128)(2,1)} %param.28) | copy-start | bytes 196612
  6.5 3.7 copy-start.5
  6.5 78.5 %all-gather.9.cloned.1.call-start = ((), (), s32[]{:S(2)}) async-start(), calls=%async_computation.3 | async-start | bytes 9175040 | tf_op jit(solution)/shard_map/all_gather | solution.py:37
  9.5 8.7 %copy-start.7 = (f32[2048]{0:T(1024)S(1)}, f32[2048]{0:T(1024)}, u32[]{:S(2)}) copy-start(f32[2048]{0:T(1024)} %param.20) | copy-start | bytes 24580
  9.5 108.8 %all-gather.17.cloned.1.call-start = ((), (), s32[]{:S(2)}) async-start(), calls=%async_computation.7 | async-start | bytes 2621440 | tf_op jit(solution)/shard_map/all_gather | solution.py:188
  11.9 8.1 %all-to-all-start = ((bf16[2,1,512,1024]{3,2,1,0:T(8,128)(2,1)}), bf16[2,1,512,1024]{3,2,1,0:T(8,128)(2,1)}, u32[]{:S(2)}, u32[]{:S(2)}) async-start(bf16[2,1,512,1024]{3,2,1,0:T(8,128)(2,1)} %broadcast_in_dim.182), calls=%async_computation | async-start | bytes 4194304 | tf_op jit(solution)/shard_map/all_to_all | solution.py:19
  17.4 124.8 %all-gather.11.cloned.1.call-start = ((), (), s32[]{:S(2)}) async-start(), calls=%async_computation.4 | async-start | bytes 1310720 | tf_op jit(solution)/shard_map/all_gather | solution.py:187
  18.1 250.4 %all-gather.15.cloned.1.call-start = ((), (), s32[]{:S(2)}) async-start(), calls=%async_computation.6 | async-start | bytes 17825792 | tf_op jit(solution)/shard_map/all_gather | solution.py:153
  92.9 3.7 copy-start.11
  92.9 3.9 copy-start.3
  100.9 646.1 %all-gather.19.cloned.1.call-start = ((), (), s32[]{:S(2)}) async-start(), calls=%async_computation.8 | async-start | bytes 6291456 | tf_op jit(solution)/shard_map/all_gather | solution.py:196
  118.3 632.2 %all-gather.13.cloned.1.call-start = ((), (), s32[]{:S(2)}) async-start(), calls=%async_computation.5 | async-start | bytes 3145728 | tf_op jit(solution)/shard_map/all_gather | solution.py:195
  121.2 3.7 copy-start.12
  121.2 4.6 copy-start.4
  124.9 4.3 copy-start.13
  124.9 6.9 copy-start.10
  125.2 17.1 %collective-permute-start.1 = (bf16[256,8,64]{0,2,1:T(8,128)(2,1)S(1)}, bf16[256,8,64]{0,2,1:T(8,128)(2,1)S(1)}, u32[]{:S(2)}, u32[]{:S(2)}) collective-permute-start(bf16[256,8,64]{0,2,1:T(8,128)(2,1)S(1)} %get-tuple-element.132), channel_id=1, source_target_pairs={{0,8},{8,0},{16,24},{24,16},{32,40},{40,32},{48,56},{56,48},{64,72... | collective-permute-start | bytes 786440 | tf_op jit(solution)/shard_map/ppermute | solution.py:51
  127.9 14.4 %collective-permute-start = (bf16[16,256]{1,0:T(8,128)(2,1)S(1)}, bf16[16,256]{1,0:T(8,128)(2,1)S(1)}, u32[]{:S(2)}, u32[]{:S(2)}) collective-permute-start(bf16[16,256]{1,0:T(8,128)(2,1)S(1)} %slice.170), channel_id=1, source_target_pairs={{0,8},{8,16},{16,24},{24,32},{32,40},{40,48},{48,56},{56,64},{64,7... | collective-permute-start | bytes 24584 | tf_op jit(solution)/shard_map/ppermute | solution.py:47
  142.3 10.9 %collective-permute-start.2 = (bf16[256,8,64]{0,2,1:T(8,128)(2,1)S(1)}, bf16[256,8,64]{0,2,1:T(8,128)(2,1)S(1)}, u32[]{:S(2)}, u32[]{:S(2)}) collective-permute-start(bf16[256,8,64]{0,2,1:T(8,128)(2,1)S(1)} %collective-permute-done.1), channel_id=1, source_target_pairs={{0,16},{8,24},{16,0},{24,8},{32,48},{40,56},{48,32},{56,40},{64,80... | collective-permute-start | bytes 786440 | tf_op jit(solution)/shard_map/ppermute | solution.py:51
  143.6 2.3 copy-start.9
  146.6 123.7 %copy-start.14 = (f32[8]{0:T(128)S(1)}, f32[8]{0:T(128)}, u32[]{:S(2)}) copy-start(f32[8]{0:T(128)} %param.27) | copy-start | bytes 100
  146.6 7.8 %all-to-all-start.1 = ((bf16[2,256,256]{2,1,0:T(8,128)(2,1)}), bf16[2,256,256]{2,1,0:T(8,128)(2,1)S(1)}, u32[]{:S(2)}, u32[]{:S(2)}) async-start(bf16[2,256,256]{2,1,0:T(8,128)(2,1)} %multiply_convert_fusion.3), calls=%async_computation.1 | async-start | bytes 524288 | tf_op jit(solution)/shard_map/all_to_all | solution.py:191
  153.2 9.7 %collective-permute-start.3 = (bf16[256,8,64]{0,2,1:T(8,128)(2,1)S(1)}, bf16[256,8,64]{0,2,1:T(8,128)(2,1)S(1)}, u32[]{:S(2)}, u32[]{:S(2)}) collective-permute-start(bf16[256,8,64]{0,2,1:T(8,128)(2,1)S(1)} %collective-permute-done.2), channel_id=1, source_target_pairs={{0,32},{8,40},{16,48},{24,56},{32,0},{40,8},{48,16},{56,24},{64,96... | collective-permute-start | bytes 786440 | tf_op jit(solution)/shard_map/ppermute | solution.py:51
  162.8 7.3 collective-permute-start.4
  270.3 10.6 %copy-start.2 = (f32[8,256,512]{2,1,0:T(8,128)}, f32[8,256,512]{2,1,0:T(8,128)S(1)}, u32[]{:S(2)}) copy-start(f32[8,256,512]{2,1,0:T(8,128)S(1)} %fusion.97) | copy-start | bytes 12582916
  311.4 19.0 %collective-permute-start.5 = (bf16[256,512]{0,1:T(8,128)(2,1)S(1)}, bf16[256,512]{0,1:T(8,128)(2,1)S(1)}, u32[]{:S(2)}, u32[]{:S(2)}) collective-permute-start(bf16[256,512]{0,1:T(8,128)(2,1)S(1)} %bitcast.254), channel_id=1, source_target_pairs={{0,8},{8,0},{16,24},{24,16},{32,40},{40,32},{48,56},{56,48},{64,72... | collective-permute-start | bytes 786440 | tf_op jit(solution)/shard_map/ppermute | solution.py:51
  330.5 37.9 %collective-permute-start.6 = (bf16[256,512]{0,1:T(8,128)(2,1)S(1)}, bf16[256,512]{0,1:T(8,128)(2,1)S(1)}, u32[]{:S(2)}, u32[]{:S(2)}) collective-permute-start(bf16[256,512]{0,1:T(8,128)(2,1)S(1)} %collective-permute-done.5), channel_id=1, source_target_pairs={{0,16},{8,24},{16,0},{24,8},{32,48},{40,56},{48,32},{56,40},{64,80... | collective-permute-start | bytes 786440 | tf_op jit(solution)/shard_map/ppermute | solution.py:51
  368.3 59.7 %collective-permute-start.7 = (bf16[256,512]{0,1:T(8,128)(2,1)S(1)}, bf16[256,512]{0,1:T(8,128)(2,1)S(1)}, u32[]{:S(2)}, u32[]{:S(2)}) collective-permute-start(bf16[256,512]{0,1:T(8,128)(2,1)S(1)} %collective-permute-done.6), channel_id=1, source_target_pairs={{0,32},{8,40},{16,48},{24,56},{32,0},{40,8},{48,16},{56,24},{64,96... | collective-permute-start | bytes 786440 | tf_op jit(solution)/shard_map/ppermute | solution.py:51
  428.0 310.9 %collective-permute-start.8 = (bf16[256,512]{0,1:T(8,128)(2,1)S(1)}, bf16[256,512]{0,1:T(8,128)(2,1)S(1)}, u32[]{:S(2)}, u32[]{:S(2)}) collective-permute-start(bf16[256,512]{0,1:T(8,128)(2,1)S(1)} %collective-permute-done.7), channel_id=1, source_target_pairs={{0,64},{8,72},{16,80},{24,88},{32,96},{40,104},{48,112},{56,120},{... | collective-permute-start | bytes 786440 | tf_op jit(solution)/shard_map/ppermute | solution.py:51
  738.8 8.0 %copy-start.8 = (f32[2,1,512]{2,1,0:T(1,128)S(1)}, f32[2,1,512]{2,1,0:T(1,128)}, u32[]{:S(2)}) copy-start(f32[2,1,512]{2,1,0:T(1,128)} %convert_element_type.154) | copy-start | bytes 12292
  746.8 3.8 copy-start.6
  747.0 6.8 copy-start.1
Sparse Core Ops, SparseCore 0:
  9.6 75.4 all-gather.8
  86.7 31.5 all-gather.16
  120.0 22.1 all-gather.10
  144.2 124.2 all-gather.14
  270.0 19.9 all-gather.18
  291.5 14.6 all-gather.12
where the time goes:
time: 772 us; the launch traced here: 761 us
  starting transfers between devices  224 us (29%)
  waiting for transfers between devices  201 us (26%)
  matrix products  178 us (23%)
  other arithmetic  68 us (9%)
  local copies, waits for them, and re-layouts  63.1 us (8%)
  between operations  14.2 us (2%)
  blocking collectives  11.4 us (1%)
    ppermute x8, starting transfers between devices, partner_2(): lax.ppermute(shard, axis, [(i, i ^ 1 << distance) for i in range(lax.axis...  210 us
    all_gather x1, waiting for transfers between devices, shards(): everything = lax.all_gather(key_value, 'sp', axis=1, tiled=True)  98.3 us
    dot_general x17, matrix products, stick_block(): jnp.einsum('htk,khd->thd', weight, value_heads, preferred_element_type=jn...  84 us
    dot_general x17, matrix products, stick_block(): jnp.einsum('thd,khd->htk', query, key_heads, preferred_element_type=jnp.f...  73.3 us
    another operation x52, other arithmetic  57.9 us
    all_gather x1, waiting for transfers between devices, in_one_piece(): whole, at, outs = (lax.all_gather(both, axis, axis=dim, tiled=True), 0, [])  57.7 us
    another operation x36, local copies, waits for them, and re-layouts  42.3 us
    all_gather x1, waiting for transfers between devices, shards(): lax.all_gather(w_out_attn, 'fs', axis=1, tiled=True)  17.3 us
  transfers between devices with their start and end apart: 17, of which 9 were waited for; matrix products, arithmetic and copies ran while one was open for 40% of the time, Pallas kernels for 0%

commit v1 on v0

v1 whole, which is shorter than its diff:
```python
import functools
import math

import jax
import jax.numpy as jnp
from jax import lax
from jax.experimental import pallas as pl
from jax.experimental.pallas import tpu as pltpu
from jax.sharding import PartitionSpec as P

HEADS = 16
HEAD_DIM = 64
POOL = 512
POOL_GROUPS = 4
BLOCKS = 16
HALF = 256
BLOCK = 512

EPS = 1e-06
LOG2E = 1.4426950408889634


def sent_to_all(shard, axis):
    devices = lax.axis_size(axis)
    return lax.all_to_all(
        jnp.broadcast_to(shard[None], (devices, *shard.shape)), axis, 0, 0, tiled=True
    )


def in_order(parts, dim):
    lengths = list(parts.shape[1:])
    lengths[dim] *= parts.shape[0]
    return jnp.moveaxis(parts, 0, dim).reshape(lengths)


def gathered_copies(shard, axis, dim):
    parts = sent_to_all(shard, axis)
    return in_order(parts, dim)


def shifted_2(value, axis, steps):
    count = lax.axis_size(axis)
    initial, last = (max(0, -steps), min(count, count - steps))
    return lax.ppermute(value, axis, [(source, source + steps) for source in range(initial, last)])


def branch_norm(values_in, squares, width, gain):
    values_f = values_in.astype(jnp.float32)
    factor = lax.rsqrt(squares / width + EPS)
    return (values_f * factor[:, None] * gain.astype(jnp.float32)).astype(jnp.bfloat16)


def split_terms(value):
    high = value.astype(jnp.bfloat16)
    rest = value - high.astype(jnp.float32)
    middle = rest.astype(jnp.bfloat16)
    low = (rest - middle.astype(jnp.float32)).astype(jnp.bfloat16)
    return (high, middle, low)


def attention_kernel(half_ref, offset_ref, x_ref, o_ref, q_s, k_s, v_s, tri_s, acc_s, carry_s, z0, z1, l0, l1):
    scale = LOG2E / math.sqrt(HEAD_DIM)
    half = half_ref[0]
    offset = offset_ref[0] * math.sqrt(HEAD_DIM)

    row16 = lax.broadcasted_iota(jnp.int32, (64, BLOCK), 0)
    terms = split_terms(jnp.full((64, BLOCK), offset, jnp.float32))
    extra = jnp.where(
        row16 == 0,
        terms[0].astype(jnp.float32),
        jnp.where(
            row16 == 1,
            terms[1].astype(jnp.float32),
            jnp.where(row16 == 2, terms[2].astype(jnp.float32), 0.0),
        ),
    ).astype(jnp.bfloat16)
    lane = lax.broadcasted_iota(jnp.int32, (HALF, 64), 1)
    ones = jnp.where(lane < 3, 1.0, 0.0).astype(jnp.bfloat16)
    tri_s[...] = jnp.where(
        lax.broadcasted_iota(jnp.int32, (HALF, HALF), 0)
        >= lax.broadcasted_iota(jnp.int32, (HALF, HALF), 1),
        1.0,
        0.0,
    ).astype(jnp.bfloat16)

    def prepare(r, unused):
        k_s[r, 0:64, 0:HALF] = x_ref[r, 0:64, :]
        k_s[r, 0:64, HALF:BLOCK] = x_ref[r, 128:192, :]
        k_s[r, 64:128, :] = extra
        v_s[r, 0:HALF, :] = x_ref[r, 64:128, :].astype(jnp.float32).T.astype(jnp.bfloat16)
        v_s[r, HALF:BLOCK, :] = x_ref[r, 192:256, :].astype(jnp.float32).T.astype(jnp.bfloat16)
        q_s[r, :, 0:64] = x_ref[r, 256:320, :].astype(jnp.float32).T.astype(jnp.bfloat16)
        q_s[r, :, 64:128] = ones
        return unused

    lax.fori_loop(0, BLOCKS, prepare, 0)

    def scores(r, g, z_ref, l_ref, masked):
        z = (
            jnp.dot(q_s[r], k_s[g], preferred_element_type=jnp.float32) * scale
        )
        soft = jnp.log2(1.0 + jnp.exp2(z))
        if masked:
            earlier = (
                lax.broadcasted_iota(jnp.int32, (HALF, BLOCK), 1)
                < lax.broadcasted_iota(jnp.int32, (HALF, BLOCK), 0) + half * HALF
            )
            soft = jnp.where(earlier, soft, 0.0)
            z = jnp.where(earlier, z, -1e30)
        z_ref[...] = z
        l_ref[...] = soft.astype(jnp.bfloat16)

    def weigh(r, g, z_ref, l_ref, first):
        late = jnp.dot(l_ref[:, HALF:], tri_s[...], preferred_element_type=jnp.float32)
        early = jnp.dot(l_ref[:, :HALF], tri_s[...], preferred_element_type=jnp.float32)
        late_total = late[:, 0:1]
        early_total = early[:, 0:1]
        if first:
            w_late = jnp.exp2(z_ref[:, HALF:] - late)
            before = late_total
        else:
            carry = carry_s[r][:, 0:1]
            w_late = jnp.exp2(z_ref[:, HALF:] - (late + carry))
            before = carry + late_total
        w_early = jnp.exp2(z_ref[:, :HALF] - (early + before))
        w = jnp.concatenate([w_early.astype(jnp.bfloat16), w_late.astype(jnp.bfloat16)], axis=1)
        out = jnp.dot(w, v_s[g], preferred_element_type=jnp.float32)
        carry_s[r] = jnp.broadcast_to(before + early_total, (HALF, 128))
        if first:
            acc_s[r] = out
        else:
            acc_s[r] = acc_s[r] + out

    scores(0, 0, z0, l0, True)

    def own(n, unused):
        r = 2 * n
        scores(r + 1, r + 1, z1, l1, True)
        weigh(r, r, z0, l0, True)
        after = jnp.minimum(r + 2, BLOCKS - 1)
        scores(after, after, z0, l0, True)
        weigh(r + 1, r + 1, z1, l1, True)
        return unused

    lax.fori_loop(0, BLOCKS // 2, own, 0)

    def advance(state):
        distance, r = state
        over = r == BLOCKS - 1
        distance = jnp.where(over, distance + 1, distance)
        r = jnp.where(over, distance, r + 1)
        fits = r < BLOCKS
        return (jnp.where(fits, distance, BLOCKS - 1), jnp.where(fits, r, BLOCKS - 1))

    start = (jnp.int32(1), jnp.int32(1))
    scores(1, 0, z0, l0, False)

    def earlier_blocks(n, state):
        after = advance(state)
        last = advance(after)
        scores(after[1], after[1] - after[0], z1, l1, False)
        weigh(state[1], state[1] - state[0], z0, l0, False)
        scores(last[1], last[1] - last[0], z0, l0, False)
        weigh(after[1], after[1] - after[0], z1, l1, False)
        return last

    lax.fori_loop(0, BLOCKS * (BLOCKS - 1) // 4, earlier_blocks, start)

    def finish(r, unused):
        o_ref[r] = acc_s[r].T.astype(jnp.bfloat16)
        return unused

    lax.fori_loop(0, BLOCKS, finish, 0)


def attention(half, offset, packed):
    return pl.pallas_call(
        attention_kernel,
        out_shape=jax.ShapeDtypeStruct((BLOCKS, HEAD_DIM, HALF), jnp.bfloat16),
        in_specs=[
            pl.BlockSpec(memory_space=pltpu.SMEM),
            pl.BlockSpec(memory_space=pltpu.SMEM),
            pl.BlockSpec(memory_space=pltpu.VMEM),
        ],
        out_specs=pl.BlockSpec(memory_space=pltpu.VMEM),
        scratch_shapes=[
            pltpu.VMEM((BLOCKS, HALF, 128), jnp.bfloat16),
            pltpu.VMEM((BLOCKS, 128, BLOCK), jnp.bfloat16),
            pltpu.VMEM((BLOCKS, BLOCK, HEAD_DIM), jnp.bfloat16),
            pltpu.VMEM((HALF, HALF), jnp.bfloat16),
            pltpu.VMEM((BLOCKS, HALF, HEAD_DIM), jnp.float32),
            pltpu.VMEM((BLOCKS, HALF, 128), jnp.float32),
            pltpu.VMEM((HALF, BLOCK), jnp.float32),
            pltpu.VMEM((HALF, BLOCK), jnp.float32),
            pltpu.VMEM((HALF, BLOCK), jnp.bfloat16),
            pltpu.VMEM((HALF, BLOCK), jnp.bfloat16),
        ],
        compiler_params=pltpu.CompilerParams(vmem_limit_bytes=48 * 1024 * 1024),
        cost_estimate=pl.CostEstimate(
            flops=40_000_000_000, bytes_accessed=4_000_000, transcendentals=50_000_000
        ),
        name="stick_attention",
    )(half, offset, packed)


def head_norm_t(projected, gain):
    factor = lax.rsqrt(jnp.mean(projected * projected, axis=1, keepdims=True) + EPS)
    return (projected * factor * gain[None, :, None]).astype(jnp.bfloat16)


def pooling(pool_raw, pool_mix, pool_scale):
    row_count, pool_cols = pool_raw.shape
    reach = 16
    pool_in = pool_raw.astype(jnp.bfloat16)
    previous = shifted_2(pool_in[row_count - reach :], "sp", 1)
    extended = jnp.concatenate([previous, pool_in], axis=0).astype(jnp.float32)
    group_ch = POOL // POOL_GROUPS
    local_groups = pool_cols // group_ch
    group_ids = (
        lax.axis_index("tp") * local_groups + jnp.arange(pool_cols, dtype=jnp.int32) // group_ch
    )
    window = jnp.left_shift(jnp.int32(2), group_ids)
    summed = jnp.zeros((row_count, pool_cols), jnp.float32)
    for behind in range(reach):
        shifted = extended[reach - behind : reach - behind + row_count]
        summed = summed + jnp.where(behind < window[None, :], shifted, 0.0)
    sp_index = lax.axis_index("sp")
    position = sp_index * row_count + jnp.arange(row_count, dtype=jnp.int32)
    counted = jnp.minimum(position[:, None] + 1, window[None, :]).astype(jnp.float32)
    centered = (summed / counted - extended[reach:]).astype(jnp.bfloat16)
    pooled = jnp.einsum(
        "tgc,gcd->tgd",
        centered.reshape(row_count, local_groups, group_ch),
        pool_mix,
        preferred_element_type=jnp.float32,
    )
    return (pooled.reshape(row_count, pool_cols) * pool_scale).astype(jnp.bfloat16)


def shards(
    tokens,
    norm_gain,
    w_pool_in,
    w_query,
    w_key,
    w_value,
    query_gain,
    key_gain,
    stick_offset,
    pool_mix,
    pool_scale,
    pool_gain,
    attn_gain,
    w_out_pool,
    w_out_attn,
):
    sp_index = lax.axis_index("sp")
    whole = gathered_copies(tokens, "tp", 2)[0]
    whole_f = whole.astype(jnp.float32)
    normed = (
        whole_f * lax.rsqrt(jnp.mean(whole_f * whole_f, axis=-1, keepdims=True) + EPS) * norm_gain
    ).astype(jnp.bfloat16)
    both = jnp.concatenate((w_query, w_key, w_value, w_pool_in), axis=1)
    weights = lax.all_gather(both, "fs", axis=0, tiled=True)
    pool_raw = jnp.dot(normed, weights[:, 1536:], preferred_element_type=jnp.float32)
    raw = lax.dot_general(
        weights[:, :1536], normed, (((0,), (1,)), ((), ())), preferred_element_type=jnp.float32
    ).reshape(3, 8, HEAD_DIM, BLOCK)
    query = head_norm_t(raw[0], query_gain)
    key = head_norm_t(raw[1], key_gain)
    value = raw[2].astype(jnp.bfloat16)
    key_value = jnp.concatenate(
        [key[:, :, :HALF], value[:, :, :HALF], key[:, :, HALF:], value[:, :, HALF:]], axis=1
    )
    packed = jnp.stack(
        [
            jnp.concatenate([key_value, query[:, :, :HALF]], axis=1),
            jnp.concatenate([key_value, query[:, :, HALF:]], axis=1),
        ],
        axis=1,
    ).reshape(BLOCKS, 5 * HEAD_DIM, HALF)
    packed = lax.all_to_all(packed, "sp", 0, 0, tiled=True)
    offset = lax.dynamic_slice_in_dim(stick_offset, sp_index // 2, 1, 0)
    half = jnp.reshape(sp_index % 2, (1,))
    attended = attention(half, offset, packed)
    attended = lax.all_to_all(attended, "sp", 0, 0, tiled=True)
    attn_out = (
        attended.reshape(8, 2, HEAD_DIM, HALF).transpose(0, 2, 1, 3).reshape(8 * HEAD_DIM, 2, HALF)
    )
    pool_out = pooling(pool_raw, pool_mix, pool_scale)
    w_pool_cols, w_attn_cols = (
        lax.all_gather(w_out_pool, "fs", axis=1, tiled=True),
        lax.all_gather(w_out_attn, "fs", axis=1, tiled=True),
    )
    pool_rows = lax.all_to_all(pool_out, "tp", split_axis=0, concat_axis=1, tiled=True)
    attn_cols = lax.all_to_all(
        jnp.moveaxis(attn_out, 1, 0), "tp", split_axis=0, concat_axis=0, tiled=True
    ).reshape(2 * 8 * HEAD_DIM, HALF)
    w_pool_all, w_attn_all, pool_gain_all, attn_gain_all = (
        lax.all_gather(w_pool_cols, "tp", axis=0, tiled=True),
        lax.all_gather(w_attn_cols, "tp", axis=0, tiled=True),
        lax.all_gather(pool_gain, "tp", axis=0, tiled=True),
        lax.all_gather(attn_gain, "tp", axis=0, tiled=True),
    )
    pool_f = pool_rows.astype(jnp.float32)
    attn_f = attn_cols.astype(jnp.float32)
    pool_normed = branch_norm(pool_rows, jnp.sum(pool_f * pool_f, axis=-1), POOL, pool_gain_all)
    factor = lax.rsqrt(jnp.sum(attn_f * attn_f, axis=0) / (HEADS * HEAD_DIM) + EPS)
    attn_normed = (
        attn_f * factor[None, :] * attn_gain_all.astype(jnp.float32)[:, None]
    ).astype(jnp.bfloat16)
    mixed = jnp.dot(pool_normed, w_pool_all, preferred_element_type=jnp.float32) + lax.dot_general(
        attn_normed, w_attn_all, (((0,), (0,)), ((), ())), preferred_element_type=jnp.float32
    )
    return mixed.astype(jnp.bfloat16)[None]


def solution(mesh):
    in_specs = (
        P("fs", "sp", "tp"),
        P(),
        P("fs", "tp"),
        P("fs", "tp"),
        P("fs", "tp"),
        P("fs", "tp"),
        P(),
        P(),
        P("tp"),
        P("tp", None, None),
        P("tp"),
        P("tp"),
        P("tp"),
        P("tp", "fs"),
        P("tp", "fs"),
    )
    out_specs = P("fs", ("sp", "tp"), None)
    return jax.shard_map(shards, mesh=mesh, in_specs=in_specs, out_specs=out_specs, check_vma=False)
```

time: 772 us -> 285 us (0.37)
  the two profiles are of different devices: /device:TPU:103 before, /device:TPU:1 now
where the time goes in v1:
time: 285 us
  waiting for transfers between devices  145 us (51%)
  Pallas kernels  64.9 us (23%)
  starting transfers between devices  18.7 us (7%)
  matrix products  15.7 us (6%)
  blocking collectives  14.9 us (5%)
  between operations  13.5 us (5%)
  other arithmetic  7.78 us (3%)
  local copies, waits for them, and re-layouts  4.2 us (1%)
    all_gather x1, waiting for transfers between devices, shards(): weights = lax.all_gather(both, 'fs', axis=0, tiled=True)  76 us
    pallas_call x1, Pallas kernels, attention(): pl.pallas_call(attention_kernel, out_shape=jax.ShapeDtypeStruct((BLOCKS,...  64.9 us
    all_to_all x1, waiting for transfers between devices, shards(): packed = lax.all_to_all(packed, 'sp', 0, 0, tiled=True)  35.1 us
    all_gather x1, waiting for transfers between devices, shards(): lax.all_gather(w_out_attn, 'fs', axis=1, tiled=True)  21.2 us
    all_to_all x1, waiting for transfers between devices, shards(): attended = lax.all_to_all(attended, 'sp', 0, 0, tiled=True)  9.56 us
    all_to_all x1, starting transfers between devices, shards(): packed = lax.all_to_all(packed, 'sp', 0, 0, tiled=True)  6.51 us
    all_to_all x1, blocking collectives, shards(): lax.all_to_all(jnp.moveaxis(attn_out, 1, 0), 'tp', split_axis=0, concat_a...  6.22 us
  transfers between devices with their start and end apart: 9, of which 5 were waited for; matrix products, arithmetic and copies ran while one was open for 9% of the time, Pallas kernels for 23%

profile of v1, /device:TPU:1, one launch (start us, length us, event | category | flops | bytes accessed | tf_op | source)
XLA Modules:
  0.0 284.7 jit_solution(9246902786638502932)
XLA Ops:
  6.5 0.7 all-gather.14.cloned.1.call-update
  7.3 2.8 pad_maximum_fusion.1
  10.2 0.5 copy.24
  10.7 1.6 broadcast_in_dim.144
  12.3 5.1 %all-to-all-start = ((bf16[2,1,512,1024]{2,3,1,0:T(8,128)(2,1)}), bf16[2,1,512,1024]{2,3,1,0:T(8,128)(2,1)S(1)}, u32[]{:S(2)}, u32[]{:S(2)}) async-start(bf16[2,1,512,1024]{2,3,1,0:T(8,128)(2,1)} %broadcast_in_dim.144), calls=%async_computation | async-start | bytes 4194304 | tf_op jit(solution)/shard_map/all_to_all | solution.py:25
  17.4 0.7 all-gather.10.cloned.1.call-update
  18.4 1.6 all-to-all-done
  19.9 0.5 multiply_reduce_fusion
  20.5 0.6 bitcast_convert_fusion
  21.2 0.5 fusion.3
  21.6 21.2 %all-gather.14.cloned.1.call-done = bf16[512,2048]{1,0:T(8,128)(2,1)} async-done(((bf16[512,512]{1,0:T(8,128)(2,1)}), bf16[512,2048]{1,0:T(8,128)(2,1)}) %all-gather.14.cloned.1.call-update) | async-done | bytes 2097168 | tf_op jit(solution)/shard_map/all_gather | solution.py:293
  42.9 76.0 %all-gather.8.cloned.1.call-done = bf16[2048,1792]{1,0:T(8,128)(2,1)} async-done(((bf16[512,1792]{1,0:T(8,128)(2,1)}), bf16[2048,1792]{1,0:T(8,128)(2,1)}) %all-gather.8.cloned.1.call-update) | async-done | bytes 7340048 | tf_op jit(solution)/shard_map/all_gather | solution.py:264
  118.9 5.5 %fusion = f32[1536,512]{1,0:T(8,128)S(1)} fusion(bf16[512,2048]{0,1:T(8,128)(2,1)S(1)} %fusion.3, bf16[2048,1792]{1,0:T(8,128)(2,1)} %all-gather.8.cloned.1.call-done), kind=kOutput, calls=%fused_computation | convolution fusion | flops 3221225472 | bytes 11534336 | tf_op jit(solution)/shard_map/dot_general | solution.py:266
  124.9 2.0 convolution_convert_fusion
  126.9 3.1 %collective-permute-start = (bf16[16,256]{1,0:T(8,128)(2,1)S(1)}, bf16[16,256]{1,0:T(8,128)(2,1)S(1)}, u32[]{:S(2)}, u32[]{:S(2)}) collective-permute-start(bf16[16,256]{1,0:T(8,128)(2,1)S(1)} %slice.118), channel_id=1, source_target_pairs={{0,8},{8,16},{16,24},{24,32},{32,40},{40,48},{48,56},{56,64},{64,7... | collective-permute-start | bytes 24584 | tf_op jit(solution)/shard_map/ppermute | solution.py:44
  130.0 0.5 multiply_convert_fusion
  130.7 1.7 pad_maximum_fusion
  132.5 1.4 convolution_bitcast_fusion
  134.0 0.4 copy.27
  134.4 0.4 reshape.171
  134.9 4.7 %all_to_all.30 = bf16[2,256,256]{2,1,0:T(8,128)(2,1)S(1)} all-to-all(bf16[2,256,256]{2,1,0:T(8,128)(2,1)S(1)} %multiply_convert_fusion.2), channel_id=1, replica_groups=mesh['sp'=16,'fs'=4,'tp'=2] {'tp'}, dimensions={0} | all-to-all | bytes 524288 | tf_op jit(solution)/shard_map/all_to_all | solution.py:295
  139.6 6.5 %all-to-all-start.2 = ((bf16[16,320,256]{2,1,0:T(8,128)(2,1)}), bf16[16,320,256]{2,1,0:T(8,128)(2,1)S(1)}, u32[]{:S(2)}, u32[]{:S(2)}) async-start(bf16[16,320,256]{2,1,0:T(8,128)(2,1)} %bitcast.66), calls=%async_computation.2 | async-start | bytes 5242880 | tf_op jit(solution)/shard_map/all_to_all | solution.py:282
  146.2 2.1 all-gather
  148.3 1.8 all-gather.1
  150.1 0.6 dynamic_slice.3.offset_ref
  150.8 35.1 %all-to-all-done.2.x_ref = bf16[16,320,256]{2,1,0:T(8,128)(2,1)S(1)} async-done(((bf16[16,320,256]{2,1,0:T(8,128)(2,1)}), bf16[16,320,256]{2,1,0:T(8,128)(2,1)S(1)}, u32[]{:S(2)}, u32[]{:S(2)}) %all-to-all-start.2) | async-done | bytes 2621472 | tf_op jit(solution)/shard_map/all_to_all | solution.py:282
  185.9 64.9 %stick_attention.1 = bf16[16,64,256]{2,1,0:T(8,128)(2,1)} custom-call(s32[1]{0:T(128)} %bitcast.8.half_ref, f32[1]{0:T(128)} %dynamic_slice.3.offset_ref, bf16[16,320,256]{2,1,0:T(8,128)(2,1)S(1)} %all-to-all-done.2.x_ref), custom_call_target="tpu_custom_call" | custom-call | flops 40000000000 | bytes 4000000 | tf_op jit(solution)/shard_map/stick_attention/pallas_call | solution.py:177
  250.8 3.8 %all-to-all-start.3 = ((bf16[16,64,256]{2,1,0:T(8,128)(2,1)}), bf16[16,64,256]{2,1,0:T(8,128)(2,1)S(1)}, u32[]{:S(2)}, u32[]{:S(2)}) async-start(bf16[16,64,256]{2,1,0:T(8,128)(2,1)} %stick_attention.1), calls=%async_computation.3 | async-start | bytes 1048576 | tf_op jit(solution)/shard_map/all_to_all | solution.py:286
  255.1 9.6 %all-to-all-done.3 = bf16[16,64,256]{2,1,0:T(8,128)(2,1)S(1)} async-done(((bf16[16,64,256]{2,1,0:T(8,128)(2,1)}), bf16[16,64,256]{2,1,0:T(8,128)(2,1)S(1)}, u32[]{:S(2)}, u32[]{:S(2)}) %all-to-all-start.3) | async-done | bytes 524320 | tf_op jit(solution)/shard_map/all_to_all | solution.py:286
  264.8 6.2 %all_to_all.31 = bf16[2,512,256]{2,1,0:T(8,128)(2,1)S(1)} all-to-all(bf16[2,512,256]{2,1,0:T(8,128)(2,1)S(1)} %bitcast.72), channel_id=1, replica_groups=mesh['sp'=16,'fs'=4,'tp'=2] {'tp'}, dimensions={0} | all-to-all | bytes 1048576 | tf_op jit(solution)/shard_map/all_to_all | solution.py:296
  271.4 3.5 %fusion.35 = f32[256,2048]{1,0:T(8,128)S(1)} fusion(bf16[1024,256]{1,0:T(8,128)(2,1)S(1)} %fusion.8, bf16[1024,2048]{1,0:T(8,128)(2,1)} %all-gather.16.cloned.1.call-done), kind=kOutput, calls=%fused_computation.106 | convolution fusion | flops 1073741824 | bytes 6815744 | tf_op jit(solution)/shard_map/dot_general | solution.py:312
  274.9 3.3 %fusion.5 = bf16[1,256,2048]{2,1,0:T(8,128)(2,1)} fusion(f32[256,2048]{1,0:T(8,128)S(1)} %fusion.35, bf16[256,512]{0,1:T(8,128)(2,1)S(1)} %fusion.28, bf16[512,2048]{1,0:T(8,128)(2,1)} %all-gather.12.cloned.1.call-done), kind=kOutput, calls=%fused_computation.9 | convolution fusion | flops 537919488 | bytes 5505024 | tf_op jit(solution)/shard_map/dot_general | solution.py:312
  (67 shorter events, 2.1 us)
Async XLA Ops:
  6.5 126.0 %copy-start = (bf16[2,128,128]{2,1,0:T(8,128)(2,1)S(1)}, bf16[2,128,128]{2,1,0:T(8,128)(2,1)}, u32[]{:S(2)}) copy-start(bf16[2,128,128]{2,1,0:T(8,128)(2,1)} %param.24) | copy-start | bytes 196612
  6.5 36.3 %all-gather.14.cloned.1.call-start = ((), (), s32[]{:S(2)}) async-start(), calls=%async_computation.8 | async-start | bytes 2621440 | tf_op jit(solution)/shard_map/all_gather | solution.py:293
  7.3 2.9 %copy-start.1 = (bf16[1,512,1024]{2,1,0:T(8,128)(2,1)S(1)}, bf16[1,512,1024]{2,1,0:T(8,128)(2,1)}, u32[]{:S(2)}) copy-start(bf16[1,512,1024]{2,1,0:T(8,128)(2,1)} %param.15) | copy-start | bytes 3145732
  7.3 111.6 %all-gather.8.cloned.1.call-start = ((), (), s32[]{:S(2)}) async-start(), calls=%async_computation.5 | async-start | bytes 9175040 | tf_op jit(solution)/shard_map/all_gather | solution.py:264
  12.3 7.6 %all-to-all-start = ((bf16[2,1,512,1024]{2,3,1,0:T(8,128)(2,1)}), bf16[2,1,512,1024]{2,3,1,0:T(8,128)(2,1)S(1)}, u32[]{:S(2)}, u32[]{:S(2)}) async-start(bf16[2,1,512,1024]{2,3,1,0:T(8,128)(2,1)} %broadcast_in_dim.144), calls=%async_computation | async-start | bytes 4194304 | tf_op jit(solution)/shard_map/all_to_all | solution.py:25
  17.4 133.3 %all-gather.10.cloned.1.call-start = ((), (), s32[]{:S(2)}) async-start(), calls=%async_computation.6 | async-start | bytes 1310720 | tf_op jit(solution)/shard_map/all_gather | solution.py:292
  18.2 253.2 %all-gather.16.cloned.1.call-start = ((), (), s32[]{:S(2)}) async-start(), calls=%async_computation.9 | async-start | bytes 6291456 | tf_op jit(solution)/shard_map/all_gather | solution.py:301
  20.5 0.7 copy-start.2
  124.8 5.2 %copy-start.5 = (f32[64]{0:T(128)S(1)}, f32[64]{0:T(128)}, u32[]{:S(2)}) copy-start(f32[64]{0:T(128)} %param.21) | copy-start | bytes 772
  124.9 5.1 %copy-start.6 = (f32[64]{0:T(128)S(1)}, f32[64]{0:T(128)}, u32[]{:S(2)}) copy-start(f32[64]{0:T(128)} %param.22) | copy-start | bytes 772
  126.9 5.6 %collective-permute-start = (bf16[16,256]{1,0:T(8,128)(2,1)S(1)}, bf16[16,256]{1,0:T(8,128)(2,1)S(1)}, u32[]{:S(2)}, u32[]{:S(2)}) collective-permute-start(bf16[16,256]{1,0:T(8,128)(2,1)S(1)} %slice.118), channel_id=1, source_target_pairs={{0,8},{8,16},{16,24},{24,32},{32,40},{40,48},{48,56},{56,64},{64,7... | collective-permute-start | bytes 24584 | tf_op jit(solution)/shard_map/ppermute | solution.py:44
  134.0 0.8 copy-start.3
  139.6 6.6 %copy-start.7 = (bf16[256]{0:T(256)(128)(2,1)S(1)}, bf16[256]{0:T(256)(128)(2,1)}, u32[]{:S(2)}) copy-start(bf16[256]{0:T(256)(128)(2,1)} %param.26) | copy-start | bytes 1540
  139.6 8.7 %copy-start.4 = (bf16[512]{0:T(512)(128)(2,1)S(1)}, bf16[512]{0:T(512)(128)(2,1)}, u32[]{:S(2)}) copy-start(bf16[512]{0:T(512)(128)(2,1)} %param.27) | copy-start | bytes 3076
  139.6 10.6 %copy-start.8 = (f32[8]{0:T(128)S(1)}, f32[8]{0:T(128)}, u32[]{:S(2)}) copy-start(f32[8]{0:T(128)} %param.23) | copy-start | bytes 100
  139.6 46.3 %all-to-all-start.2 = ((bf16[16,320,256]{2,1,0:T(8,128)(2,1)}), bf16[16,320,256]{2,1,0:T(8,128)(2,1)S(1)}, u32[]{:S(2)}, u32[]{:S(2)}) async-start(bf16[16,320,256]{2,1,0:T(8,128)(2,1)} %bitcast.66), calls=%async_computation.2 | async-start | bytes 5242880 | tf_op jit(solution)/shard_map/all_to_all | solution.py:282
  146.1 128.8 %all-gather.12.cloned.1.call-start = ((), (), s32[]{:S(2)}) async-start(), calls=%async_computation.7 | async-start | bytes 3145728 | tf_op jit(solution)/shard_map/all_gather | solution.py:300
  250.8 13.9 %all-to-all-start.3 = ((bf16[16,64,256]{2,1,0:T(8,128)(2,1)}), bf16[16,64,256]{2,1,0:T(8,128)(2,1)S(1)}, u32[]{:S(2)}, u32[]{:S(2)}) async-start(bf16[16,64,256]{2,1,0:T(8,128)(2,1)} %stick_attention.1), calls=%async_computation.3 | async-start | bytes 1048576 | tf_op jit(solution)/shard_map/all_to_all | solution.py:286
Sparse Core Ops, SparseCore 0:
  9.0 33.8 all-gather.13
  44.5 74.3 all-gather.7
  120.6 22.9 all-gather.9
  145.1 19.1 all-gather.15
  165.9 14.6 all-gather.11

commit v2 on v1

--- a/solution.py
+++ b/solution.py
@@ -20,24 +20,6 @@
 LOG2E = 1.4426950408889634
 
 
-def sent_to_all(shard, axis):
-    devices = lax.axis_size(axis)
-    return lax.all_to_all(
-        jnp.broadcast_to(shard[None], (devices, *shard.shape)), axis, 0, 0, tiled=True
-    )
-
-
-def in_order(parts, dim):
-    lengths = list(parts.shape[1:])
-    lengths[dim] *= parts.shape[0]
-    return jnp.moveaxis(parts, 0, dim).reshape(lengths)
-
-
-def gathered_copies(shard, axis, dim):
-    parts = sent_to_all(shard, axis)
-    return in_order(parts, dim)
-
-
 def shifted_2(value, axis, steps):
     count = lax.axis_size(axis)
     initial, last = (max(0, -steps), min(count, count - steps))
@@ -58,13 +40,373 @@
     return (high, middle, low)
 
 
-def attention_kernel(half_ref, offset_ref, x_ref, o_ref, q_s, k_s, v_s, tri_s, acc_s, carry_s, z0, z1, l0, l1):
+MESH = pl.DeviceIdType.MESH
+
+
+def project_kernel(
+    tok_ref, gain_ref, wk_ref, wv_ref, wq_ref, wp_ref, kg_ref, qg_ref,
+    out_ref, pool_ref,
+    buf, pbuf, tok_s, x_s, acc, acc_p, mine, theirs, send, recv,
+):
+    sp, y, core = lax.axis_index("sp"), lax.axis_index("fs"), lax.axis_index("tp")
+    z, x = sp // 4, sp % 4
+    y_up, y_down, y_far = (y + 1) % 4, (y + 3) % 4, (y + 2) % 4
+    x_up, x_down, x_far = (x + 1) % 4, (x + 3) % 4, (x + 2) % 4
+    z_up, z_down, z_far = (z + 1) % 4, (z + 3) % 4, (z + 2) % 4
+
+    def at(z_to, x_to, y_to, core_to):
+        return {"sp": z_to * 4 + x_to, "fs": y_to, "tp": core_to}
+
+    partner = at(z, x, y, 1 - core)
+    to = {
+        "yp": at(z, x, y_up, core), "ym": at(z, x, y_down, core),
+        "xp": at(z, x_up, y, core), "xm": at(z, x_down, y, core),
+        "zp": at(z_up, x, y, core), "zm": at(z_down, x, y, core),
+    }
+
+    barrier = pltpu.get_barrier_semaphore()
+    for target in (partner, *to.values()):
+        pl.semaphore_signal(barrier, inc=1, device_id=target, device_id_type=MESH)
+    pl.semaphore_wait(barrier, 7)
+
+    started = []
+
+    def remote(source, target_ref, index, target):
+        return pltpu.make_async_remote_copy(
+            src_ref=source, dst_ref=target_ref, send_sem=send.at[index],
+            recv_sem=recv.at[index], device_id=target, device_id_type=MESH,
+        )
+
+    def go(source, target_ref, index, target):
+        copy = remote(source, target_ref, index, target)
+        copy.start()
+        started.append(copy)
+
+    def got(target_ref, index):
+        remote(target_ref, target_ref, index, partner).wait_recv()
+
+    def rows(start, count=64):
+        return pl.ds(pl.multiple_of(start, 32), count)
+
+    weights = (wk_ref, wv_ref, wq_ref)
+    quarters = (y_down, y_up, y_far)
+
+    def part(a, quarter, start, count=64):
+        return buf.at[a, quarter, rows(start, count), :]
+
+    def direct(a):
+        base = a * 30
+        own_x, own_z = 64 * x, 256 + 64 * z
+        w = weights[a]
+        go(w.at[rows(own_x), :], part(a, y, own_x), base + 0, to["yp"])
+        go(w.at[rows(own_z), :], part(a, y, own_z), base + 1, to["ym"])
+        go(w.at[rows(own_x), :], part(a, y, own_x), base + 2, to["ym"])
+        go(w.at[rows(own_z), :], part(a, y, own_z), base + 3, to["yp"])
+
+    def ring_base(a, item, ring):
+        return a * 30 + 6 + item * 8 + ring * 4
+
+    own_row = (64 * x, 256 + 64 * z)
+    down_row = (64 * x_down, 256 + 64 * z_down)
+    up_row = (64 * x_up, 256 + 64 * z_up)
+    far_row = (64 * x_far, 256 + 64 * z_far)
+    ups = ("xp", "zp")
+    downs = ("xm", "zm")
+
+    def spread(a, item, ring):
+        base = ring_base(a, item, ring)
+        piece = part(a, quarters[item], own_row[ring])
+        go(piece, piece, base + 0, to[ups[ring]])
+        go(piece, piece, base + 1, to[downs[ring]])
+
+    def relay(a, item, ring):
+        base = ring_base(a, item, ring)
+        q = quarters[item]
+        got(part(a, q, down_row[ring]), base + 0)
+        piece = part(a, q, down_row[ring], 32)
+        go(piece, piece, base + 2, to[ups[ring]])
+        got(part(a, q, up_row[ring]), base + 1)
+        piece = part(a, q, up_row[ring] + 32, 32)
+        go(piece, piece, base + 3, to[downs[ring]])
+
+    def settle(a):
+        for item in range(3):
+            for ring in range(2):
+                base = ring_base(a, item, ring)
+                q = quarters[item]
+                got(part(a, q, far_row[ring], 32), base + 2)
+                got(part(a, q, far_row[ring] + 32, 32), base + 3)
+
+    def first(a):
+        base = a * 30
+        piece = part(a, y_down, own_row[0])
+        got(piece, base + 0)
+        go(piece, piece, base + 4, to["yp"])
+        spread(a, 0, 0)
+        piece = part(a, y_up, own_row[1])
+        got(piece, base + 1)
+        go(piece, piece, base + 5, to["ym"])
+        spread(a, 1, 1)
+        got(part(a, y_up, own_row[0]), base + 2)
+        spread(a, 1, 0)
+        got(part(a, y_down, own_row[1]), base + 3)
+        spread(a, 0, 1)
+
+    def second(a):
+        relay(a, 0, 0)
+        relay(a, 1, 1)
+
+    def third(a):
+        base = a * 30
+        got(part(a, y_far, own_row[0]), base + 4)
+        spread(a, 2, 0)
+        got(part(a, y_far, own_row[1]), base + 5)
+        spread(a, 2, 1)
+        relay(a, 1, 0)
+        relay(a, 0, 1)
+
+    def fourth(a):
+        relay(a, 2, 0)
+        relay(a, 2, 1)
+
+    pool_base = 90
+
+    def pool_direct():
+        go(wp_ref, pbuf.at[y], pool_base + 0, to["yp"])
+        go(wp_ref, pbuf.at[y], pool_base + 1, to["ym"])
+
+    def pool_relay():
+        got(pbuf.at[y_down], pool_base + 0)
+        piece = pbuf.at[y_down, 0:256, :]
+        go(piece, piece, pool_base + 2, to["yp"])
+        got(pbuf.at[y_up], pool_base + 1)
+        piece = pbuf.at[y_up, 256:512, :]
+        go(piece, piece, pool_base + 3, to["ym"])
+
+    def pool_settle():
+        got(pbuf.at[y_far, 0:256, :], pool_base + 2)
+        got(pbuf.at[y_far, 256:512, :], pool_base + 3)
+
+    def own(a):
+        acc[a] = jnp.dot(x_s[y], weights[a][...], preferred_element_type=jnp.float32)
+
+    def rest(a):
+        total = acc[a]
+        for q in quarters:
+            total = total + jnp.dot(x_s[q], buf[a, q], preferred_element_type=jnp.float32)
+        return total
+
+    def deliver(a, total):
+        turned = total.T.reshape(8, HEAD_DIM, BLOCK)
+        if a != 1:
+            factor = lax.rsqrt(jnp.mean(turned * turned, axis=1, keepdims=True) + EPS)
+            gain = (kg_ref if a == 0 else qg_ref)[...]
+            turned = turned * factor * gain[None]
+        turned = turned.astype(jnp.bfloat16)
+        is_first = core == 0
+        low, high = turned[:, :, :HALF], turned[:, :, HALF:]
+        out_ref[pl.ds(8 * core, 8), a * 64 : a * 64 + 64, :] = jnp.where(is_first, low, high)
+        theirs[a] = jnp.where(is_first, high, low)
+        go(
+            theirs.at[a],
+            out_ref.at[pl.ds(8 * core, 8), a * 64 : a * 64 + 64, :],
+            95 + a,
+            partner,
+        )
+
+    go(tok_ref, tok_s, 94, partner)
+    direct(0)
+    direct(1)
+    got(tok_s, 94)
+
+    mine_f = tok_ref[...].astype(jnp.float32)
+    other_f = tok_s[...].astype(jnp.float32)
+    squares = jnp.sum(mine_f * mine_f, axis=1, keepdims=True) + jnp.sum(
+        other_f * other_f, axis=1, keepdims=True
+    )
+    factor = lax.rsqrt(squares / 2048.0 + EPS)
+    for j in range(2):
+        columns = slice(512 * j, 512 * j + 512)
+        at_mine = 2 * core + j
+        at_other = 2 * (1 - core) + j
+        x_s[at_mine] = (
+            tok_ref[:, columns].astype(jnp.float32) * factor * gain_ref[at_mine]
+        ).astype(jnp.bfloat16)
+        x_s[at_other] = (
+            tok_s[:, columns].astype(jnp.float32) * factor * gain_ref[at_other]
+        ).astype(jnp.bfloat16)
+
+    first(0)
+    direct(2)
+    own(0)
+    second(0)
+    first(1)
+    pool_direct()
+    own(1)
+    third(0)
+    second(1)
+    first(2)
+    own(2)
+    fourth(0)
+    third(1)
+    second(2)
+    pool_relay()
+    acc_p[...] = jnp.dot(x_s[y], wp_ref[...], preferred_element_type=jnp.float32)
+    fourth(1)
+    third(2)
+    settle(0)
+    deliver(0, rest(0))
+    fourth(2)
+    settle(1)
+    deliver(1, rest(1))
+    settle(2)
+    deliver(2, rest(2))
+    pool_settle()
+    total = acc_p[...]
+    for q in quarters:
+        total = total + jnp.dot(x_s[q], pbuf[q], preferred_element_type=jnp.float32)
+    pool_ref[...] = total.astype(jnp.bfloat16)
+    for a in range(3):
+        got(out_ref.at[pl.ds(8 * (1 - core), 8), a * 64 : a * 64 + 64, :], 95 + a)
+    for copy in started:
+        copy.wait_send()
+
+
+def project(tokens, norm_gain, wk, wv, wq, wp, key_gain, query_gain):
+    vmem = pl.BlockSpec(memory_space=pltpu.VMEM)
+    return pl.pallas_call(
+        project_kernel,
+        out_shape=(
+            jax.ShapeDtypeStruct((HEADS, 3 * HEAD_DIM, HALF), jnp.bfloat16),
+            jax.ShapeDtypeStruct((BLOCK, 256), jnp.bfloat16),
+        ),
+        in_specs=[vmem] * 8,
+        out_specs=(vmem, vmem),
+        scratch_shapes=[
+            pltpu.VMEM((3, 4, 512, 512), jnp.bfloat16),
+            pltpu.VMEM((4, 512, 256), jnp.bfloat16),
+            pltpu.VMEM((512, 1024), jnp.bfloat16),
+            pltpu.VMEM((4, 512, 512), jnp.bfloat16),
+            pltpu.VMEM((3, 512, 512), jnp.float32),
+            pltpu.VMEM((512, 256), jnp.float32),
+            pltpu.VMEM((8, 128), jnp.float32),
+            pltpu.VMEM((3, 8, HEAD_DIM, HALF), jnp.bfloat16),
+            pltpu.SemaphoreType.DMA((98,)),
+            pltpu.SemaphoreType.DMA((98,)),
+        ],
+        compiler_params=pltpu.CompilerParams(
+            collective_id=0, has_side_effects=True, vmem_limit_bytes=56 * 1024 * 1024
+        ),
+        cost_estimate=pl.CostEstimate(
+            flops=4_000_000_000, bytes_accessed=6_000_000, transcendentals=10_000
+        ),
+        name="gather_project",
+    )(
+        tokens, norm_gain.reshape(4, 1, 512), wk, wv, wq, wp,
+        key_gain.reshape(HEAD_DIM, 1), query_gain.reshape(HEAD_DIM, 1),
+    )
+
+
+def attention_kernel(
+    offset_ref, x_ref, wp_ref, wa_ref, gains_ref,
+    o_ref, wp_all, wa_all, gains_all,
+    offset_s, other_s, q_s, k_s, v_s, tri_s, acc_s, carry_s, z0, z1, l0, l1, send, recv,
+):
+    sp, y, core = lax.axis_index("sp"), lax.axis_index("fs"), lax.axis_index("tp")
+    y_up, y_down, y_far = (y + 1) % 4, (y + 3) % 4, (y + 2) % 4
+    partner = {"sp": sp, "fs": y, "tp": 1 - core}
+    up = {"sp": sp, "fs": y_up, "tp": core}
+    down = {"sp": sp, "fs": y_down, "tp": core}
+    barrier = pltpu.get_barrier_semaphore()
+    for target in (partner, up, down):
+        pl.semaphore_signal(barrier, inc=1, device_id=target, device_id_type=MESH)
+    pl.semaphore_wait(barrier, 3)
+    started = []
+
+    def remote(source, target_ref, index, target):
+        return pltpu.make_async_remote_copy(
+            src_ref=source, dst_ref=target_ref, send_sem=send.at[index],
+            recv_sem=recv.at[index], device_id=target, device_id_type=MESH,
+        )
+
+    def go(source, target_ref, index, target):
+        copy = remote(source, target_ref, index, target)
+        copy.start()
+        started.append(copy)
+
+    def got(target_ref, index):
+        remote(target_ref, target_ref, index, partner).wait_recv()
+
+    def wa_part(quarter, of_core, start, count):
+        return wa_all.at[
+            pl.ds(pl.multiple_of(of_core * 512 + start, 128), count),
+            pl.ds(pl.multiple_of(quarter * 512, 512), 512),
+        ]
+
+    def wp_part(quarter, of_core, start, count):
+        return wp_all.at[
+            pl.ds(pl.multiple_of(of_core * 256 + start, 128), count),
+            pl.ds(pl.multiple_of(quarter * 512, 512), 512),
+        ]
+
+    def share(quarter, index):
+        go(wa_part(quarter, core, 0, 512), wa_part(quarter, core, 0, 512), index, partner)
+        go(wp_part(quarter, core, 0, 256), wp_part(quarter, core, 0, 256), index + 1, partner)
+
+    def shared(quarter, index):
+        got(wa_part(quarter, 1 - core, 0, 512), index)
+        got(wp_part(quarter, 1 - core, 0, 256), index + 1)
+
+    def weights_start():
+        go(wa_ref, wa_part(y, core, 0, 512), 2, up)
+        go(wp_ref, wp_part(y, core, 0, 256), 3, up)
+        go(wa_ref, wa_part(y, core, 0, 512), 4, down)
+        go(wp_ref, wp_part(y, core, 0, 256), 5, down)
+        go(wa_ref, wa_part(y, core, 0, 512), 10, partner)
+        go(wp_ref, wp_part(y, core, 0, 256), 11, partner)
+
+    def weights_middle():
+        got(wa_part(y_down, core, 0, 512), 2)
+        got(wp_part(y_down, core, 0, 256), 3)
+        go(wa_part(y_down, core, 0, 256), wa_part(y_down, core, 0, 256), 6, up)
+        go(wp_part(y_down, core, 0, 128), wp_part(y_down, core, 0, 128), 7, up)
+        got(wa_part(y_up, core, 0, 512), 4)
+        got(wp_part(y_up, core, 0, 256), 5)
+        go(wa_part(y_up, core, 256, 256), wa_part(y_up, core, 256, 256), 8, down)
+        go(wp_part(y_up, core, 128, 128), wp_part(y_up, core, 128, 128), 9, down)
+        share(y_down, 12)
+        share(y_up, 14)
+
+    def weights_late():
+        got(wa_part(y_far, core, 0, 256), 6)
+        got(wp_part(y_far, core, 0, 128), 7)
+        got(wa_part(y_far, core, 256, 256), 8)
+        got(wp_part(y_far, core, 128, 128), 9)
+        share(y_far, 16)
+
+    def weights_end():
+        shared(y, 10)
+        shared(y_down, 12)
+        shared(y_up, 14)
+        shared(y_far, 16)
+
+    go(offset_ref, offset_s, 18, partner)
+    keys_values = x_ref.at[:, 0:128, :]
+    go(keys_values, other_s, 0, partner)
+    go(gains_ref, gains_all.at[pl.ds(pl.multiple_of(16 * core, 16), 16), :], 1, partner)
+    weights_start()
+    wa_part(y, core, 0, 512)[...] = wa_ref[...]
+    wp_part(y, core, 0, 256)[...] = wp_ref[...]
+    gains_all[pl.ds(pl.multiple_of(16 * core, 16), 16), :] = gains_ref[...]
+
     scale = LOG2E / math.sqrt(HEAD_DIM)
-    half = half_ref[0]
-    offset = offset_ref[0] * math.sqrt(HEAD_DIM)
+    half = core
+    got(offset_s, 18)
+    of_head = jnp.where(sp // 8 == core, offset_ref[pl.ds(sp % 8, 1), :], offset_s[pl.ds(sp % 8, 1), :])
+    offset = of_head[:, 0:1] * math.sqrt(HEAD_DIM)
 
     row16 = lax.broadcasted_iota(jnp.int32, (64, BLOCK), 0)
-    terms = split_terms(jnp.full((64, BLOCK), offset, jnp.float32))
+    terms = split_terms(jnp.broadcast_to(offset, (64, BLOCK)))
     extra = jnp.where(
         row16 == 0,
         terms[0].astype(jnp.float32),
@@ -83,17 +425,29 @@
         0.0,
     ).astype(jnp.bfloat16)
 
+    mine_at = pl.ds(pl.multiple_of(core * HALF, HALF), HALF)
+    other_at = pl.ds(pl.multiple_of((1 - core) * HALF, HALF), HALF)
+
+    def turned(block):
+        return block.astype(jnp.float32).T.astype(jnp.bfloat16)
+
     def prepare(r, unused):
-        k_s[r, 0:64, 0:HALF] = x_ref[r, 0:64, :]
-        k_s[r, 0:64, HALF:BLOCK] = x_ref[r, 128:192, :]
+        k_s[r, 0:64, mine_at] = x_ref[r, 0:64, :]
         k_s[r, 64:128, :] = extra
-        v_s[r, 0:HALF, :] = x_ref[r, 64:128, :].astype(jnp.float32).T.astype(jnp.bfloat16)
-        v_s[r, HALF:BLOCK, :] = x_ref[r, 192:256, :].astype(jnp.float32).T.astype(jnp.bfloat16)
-        q_s[r, :, 0:64] = x_ref[r, 256:320, :].astype(jnp.float32).T.astype(jnp.bfloat16)
+        v_s[r, mine_at, :] = turned(x_ref[r, 64:128, :])
+        q_s[r, :, 0:64] = turned(x_ref[r, 128:192, :])
         q_s[r, :, 64:128] = ones
         return unused
 
     lax.fori_loop(0, BLOCKS, prepare, 0)
+    got(other_s, 0)
+
+    def complete(r, unused):
+        k_s[r, 0:64, other_at] = other_s[r, 0:64, :]
+        v_s[r, other_at, :] = turned(other_s[r, 64:128, :])
+        return unused
+
+    lax.fori_loop(0, BLOCKS, complete, 0)
 
     def scores(r, g, z_ref, l_ref, masked):
         z = (
@@ -164,26 +518,38 @@
         weigh(after[1], after[1] - after[0], z1, l1, False)
         return last
 
-    lax.fori_loop(0, BLOCKS * (BLOCKS - 1) // 4, earlier_blocks, start)
+    state = lax.fori_loop(0, 28, earlier_blocks, start)
+    weights_middle()
+    state = lax.fori_loop(28, 46, earlier_blocks, state)
+    weights_late()
+    lax.fori_loop(46, BLOCKS * (BLOCKS - 1) // 4, earlier_blocks, state)
 
     def finish(r, unused):
         o_ref[r] = acc_s[r].T.astype(jnp.bfloat16)
         return unused
 
     lax.fori_loop(0, BLOCKS, finish, 0)
-
-
-def attention(half, offset, packed):
+    weights_end()
+    got(gains_all.at[pl.ds(pl.multiple_of(16 * (1 - core), 16), 16), :], 1)
+    for copy in started:
+        copy.wait_send()
+
+
+def attention(offset, packed, w_pool, w_attn, gains):
+    vmem = pl.BlockSpec(memory_space=pltpu.VMEM)
     return pl.pallas_call(
         attention_kernel,
-        out_shape=jax.ShapeDtypeStruct((BLOCKS, HEAD_DIM, HALF), jnp.bfloat16),
-        in_specs=[
-            pl.BlockSpec(memory_space=pltpu.SMEM),
-            pl.BlockSpec(memory_space=pltpu.SMEM),
-            pl.BlockSpec(memory_space=pltpu.VMEM),
-        ],
-        out_specs=pl.BlockSpec(memory_space=pltpu.VMEM),
+        out_shape=(
+            jax.ShapeDtypeStruct((BLOCKS, HEAD_DIM, HALF), jnp.bfloat16),
+            jax.ShapeDtypeStruct((512, 2048), jnp.bfloat16),
+            jax.ShapeDtypeStruct((1024, 2048), jnp.bfloat16),
+            jax.ShapeDtypeStruct((32, 768), jnp.bfloat16),
+        ),
+        in_specs=[vmem] * 5,
+        out_specs=(vmem, vmem, vmem, vmem),
         scratch_shapes=[
+            pltpu.VMEM((8, 128), jnp.float32),
+            pltpu.VMEM((BLOCKS, 128, HALF), jnp.bfloat16),
             pltpu.VMEM((BLOCKS, HALF, 128), jnp.bfloat16),
             pltpu.VMEM((BLOCKS, 128, BLOCK), jnp.bfloat16),
             pltpu.VMEM((BLOCKS, BLOCK, HEAD_DIM), jnp.bfloat16),
@@ -194,24 +560,22 @@
             pltpu.VMEM((HALF, BLOCK), jnp.float32),
             pltpu.VMEM((HALF, BLOCK), jnp.bfloat16),
             pltpu.VMEM((HALF, BLOCK), jnp.bfloat16),
+            pltpu.SemaphoreType.DMA((19,)),
+            pltpu.SemaphoreType.DMA((19,)),
         ],
-        compiler_params=pltpu.CompilerParams(vmem_limit_bytes=48 * 1024 * 1024),
+        compiler_params=pltpu.CompilerParams(
+            collective_id=1, has_side_effects=True, vmem_limit_bytes=56 * 1024 * 1024
+        ),
         cost_estimate=pl.CostEstimate(
             flops=40_000_000_000, bytes_accessed=4_000_000, transcendentals=50_000_000
         ),
         name="stick_attention",
-    )(half, offset, packed)
-
-
-def head_norm_t(projected, gain):
-    factor = lax.rsqrt(jnp.mean(projected * projected, axis=1, keepdims=True) + EPS)
-    return (projected * factor * gain[None, :, None]).astype(jnp.bfloat16)
-
-
-def pooling(pool_raw, pool_mix, pool_scale):
-    row_count, pool_cols = pool_raw.shape
+    )(offset, packed, w_pool, w_attn, gains)
+
+
+def pooling(pool_in, pool_mix, pool_scale):
+    row_count, pool_cols = pool_in.shape
     reach = 16
-    pool_in = pool_raw.astype(jnp.bfloat16)
     previous = shifted_2(pool_in[row_count - reach :], "sp", 1)
     extended = jnp.concatenate([previous, pool_in], axis=0).astype(jnp.float32)
     group_ch = POOL // POOL_GROUPS
@@ -254,56 +618,22 @@
     w_out_pool,
     w_out_attn,
 ):
-    sp_index = lax.axis_index("sp")
-    whole = gathered_copies(tokens, "tp", 2)[0]
-    whole_f = whole.astype(jnp.float32)
-    normed = (
-        whole_f * lax.rsqrt(jnp.mean(whole_f * whole_f, axis=-1, keepdims=True) + EPS) * norm_gain
-    ).astype(jnp.bfloat16)
-    both = jnp.concatenate((w_query, w_key, w_value, w_pool_in), axis=1)
-    weights = lax.all_gather(both, "fs", axis=0, tiled=True)
-    pool_raw = jnp.dot(normed, weights[:, 1536:], preferred_element_type=jnp.float32)
-    raw = lax.dot_general(
-        weights[:, :1536], normed, (((0,), (1,)), ((), ())), preferred_element_type=jnp.float32
-    ).reshape(3, 8, HEAD_DIM, BLOCK)
-    query = head_norm_t(raw[0], query_gain)
-    key = head_norm_t(raw[1], key_gain)
-    value = raw[2].astype(jnp.bfloat16)
-    key_value = jnp.concatenate(
-        [key[:, :, :HALF], value[:, :, :HALF], key[:, :, HALF:], value[:, :, HALF:]], axis=1
-    )
-    packed = jnp.stack(
-        [
-            jnp.concatenate([key_value, query[:, :, :HALF]], axis=1),
-            jnp.concatenate([key_value, query[:, :, HALF:]], axis=1),
-        ],
-        axis=1,
-    ).reshape(BLOCKS, 5 * HEAD_DIM, HALF)
+    packed, pool_in = project(
+        tokens[0], norm_gain, w_key, w_value, w_query, w_pool_in, key_gain, query_gain
+    )
     packed = lax.all_to_all(packed, "sp", 0, 0, tiled=True)
-    offset = lax.dynamic_slice_in_dim(stick_offset, sp_index // 2, 1, 0)
-    half = jnp.reshape(sp_index % 2, (1,))
-    attended = attention(half, offset, packed)
-    attended = lax.all_to_all(attended, "sp", 0, 0, tiled=True)
-    attn_out = (
-        attended.reshape(8, 2, HEAD_DIM, HALF).transpose(0, 2, 1, 3).reshape(8 * HEAD_DIM, 2, HALF)
-    )
-    pool_out = pooling(pool_raw, pool_mix, pool_scale)
-    w_pool_cols, w_attn_cols = (
-        lax.all_gather(w_out_pool, "fs", axis=1, tiled=True),
-        lax.all_gather(w_out_attn, "fs", axis=1, tiled=True),
-    )
+    offset = jnp.broadcast_to(stick_offset[:, None], (8, 128))
+    gains = jnp.broadcast_to(jnp.concatenate([pool_gain, attn_gain])[None], (16, 768))
+    attended, w_pool_all, w_attn_all, gains_all = attention(
+        offset, packed, w_out_pool, w_out_attn, gains
+    )
+    attended = lax.all_to_all(attended, "sp", 0, 0, tiled=True).reshape(HEADS * HEAD_DIM, HALF)
+    pool_out = pooling(pool_in, pool_mix, pool_scale)
     pool_rows = lax.all_to_all(pool_out, "tp", split_axis=0, concat_axis=1, tiled=True)
-    attn_cols = lax.all_to_all(
-        jnp.moveaxis(attn_out, 1, 0), "tp", split_axis=0, concat_axis=0, tiled=True
-    ).reshape(2 * 8 * HEAD_DIM, HALF)
-    w_pool_all, w_attn_all, pool_gain_all, attn_gain_all = (
-        lax.all_gather(w_pool_cols, "tp", axis=0, tiled=True),
-        lax.all_gather(w_attn_cols, "tp", axis=0, tiled=True),
-        lax.all_gather(pool_gain, "tp", axis=0, tiled=True),
-        lax.all_gather(attn_gain, "tp", axis=0, tiled=True),
-    )
+    pool_gain_all = jnp.concatenate([gains_all[0, :256], gains_all[16, :256]])
+    attn_gain_all = jnp.concatenate([gains_all[0, 256:], gains_all[16, 256:]])
     pool_f = pool_rows.astype(jnp.float32)
-    attn_f = attn_cols.astype(jnp.float32)
+    attn_f = attended.astype(jnp.float32)
     pool_normed = branch_norm(pool_rows, jnp.sum(pool_f * pool_f, axis=-1), POOL, pool_gain_all)
     factor = lax.rsqrt(jnp.sum(attn_f * attn_f, axis=0) / (HEADS * HEAD_DIM) + EPS)
     attn_normed = (

time: 285 us -> 188 us (0.66)
  waiting for transfers between devices: 145 us -> 35.4 us
  Pallas kernels: 64.9 us -> 119 us
  between operations: 13.5 us -> 0.26 us
  blocking collectives: 14.9 us -> 4.42 us
  matrix products: 15.7 us -> 6.75 us
  other arithmetic: 7.78 us -> 1.84 us
  starting transfers between devices: 18.7 us -> 13 us
  local copies, waits for them, and re-layouts: 4.2 us -> 7.29 us
    all_gather x5 -> x0, waiting for transfers between devices: 97.3 us -> none  [the longest x1 76 us: shards(): weights = lax.all_gather(both, 'fs', axis=0, tiled=True)]
    pallas_call x1 -> x2, Pallas kernels: 64.9 us -> 119 us  [the longest x1 73.4 us: attention(): pl.pallas_call(attention_kernel, out_shape=(jax.ShapeDtypeStruct((BLOCKS,...]
    all_to_all x1, waiting for transfers between devices: 35.1 us -> 23.6 us  [shards(): packed = lax.all_to_all(packed, 'sp', 0, 0, tiled=True)]
    dot_general x2 -> x0, matrix products: 7.52 us -> none  [the longest x1 5.53 us: shards(): lax.dot_general(weights[:, :1536], normed, (((0,), (1,)), ((), ())), pref...]
    all_to_all x1 -> x0, blocking collectives: 6.22 us -> none  [shards(): lax.all_to_all(jnp.moveaxis(attn_out, 1, 0), 'tp', split_axis=0, concat_a...]
    all_to_all x2 -> x1, starting transfers between devices: 8.96 us -> 3.58 us  [shards(): lax.all_to_all(attended, 'sp', 0, 0, tiled=True)]
    all_gather x2 -> x0, blocking collectives: 3.95 us -> none  [the longest x1 2.11 us: shards(): lax.all_gather(pool_gain, 'tp', axis=0, tiled=True)]
    all_to_all x2 -> x1, waiting for transfers between devices: 11.1 us -> 11.2 us  [shards(): lax.all_to_all(attended, 'sp', 0, 0, tiled=True)]
  transfers between devices with their start and end apart: 9 -> 3, of which waited for: 5 -> 3; matrix products, arithmetic and copies ran while one was open for 9% -> 1% of each run, Pallas kernels for 23% -> 0%
where the time goes in v2:
time: 188 us; the launch traced here: 187 us
  Pallas kernels  119 us (63%)
  waiting for transfers between devices  35.4 us (19%)
  starting transfers between devices  13 us (7%)
  local copies, waits for them, and re-layouts  7.29 us (4%)
  matrix products  6.75 us (4%)
  blocking collectives  4.42 us (2%)
    pallas_call x1, Pallas kernels, attention(): pl.pallas_call(attention_kernel, out_shape=(jax.ShapeDtypeStruct((BLOCKS,...  73.4 us
    pallas_call x1, Pallas kernels, project(): pl.pallas_call(project_kernel, out_shape=(jax.ShapeDtypeStruct((HEADS, 3...  45.1 us
    all_to_all x1, waiting for transfers between devices, shards(): packed = lax.all_to_all(packed, 'sp', 0, 0, tiled=True)  23.6 us
    all_to_all x1, waiting for transfers between devices, shards(): lax.all_to_all(attended, 'sp', 0, 0, tiled=True)  11.2 us
    all_to_all x1, starting transfers between devices, shards(): packed = lax.all_to_all(packed, 'sp', 0, 0, tiled=True)  7.91 us
    all_to_all x1, blocking collectives, shards(): lax.all_to_all(pool_out, 'tp', split_axis=0, concat_axis=1, tiled=True)  4.42 us
  transfers between devices with their start and end apart: 3, of which 3 were waited for; matrix products, arithmetic and copies ran while one was open for 1% of the time, Pallas kernels for 0%

profile of v2, /device:TPU:1, one launch (start us, length us, event | category | flops | bytes accessed | tf_op | source)
XLA Modules:
  0.0 187.4 jit_solution(12091176404879398910)
XLA Ops:
  0.0 0.0 copy-start
  0.0 1.4 copy.20.qg_ref
  1.4 1.4 copy.19.kg_ref
  2.7 45.1 %gather_project.1 = (bf16[16,192,256]{2,1,0:T(8,128)(2,1)}, bf16[512,256]{1,0:T(8,128)(2,1)}) custom-call(bf16[512,1024]{1,0:T(8,128)(2,1)} %bitcast.36, f32[4,1,512]{2,1,0:T(1,128)} %bitcast.37, bf16[512,512]{1,0:T(8,128)(2,1)} %wk_ref.1, bf16[512,512]{1,0:T(8,128)(2,1)} %wv_ref.1, bf16[512,512]{1,0:T(8,128)(2,1)} %wq_ref.1, bf16[512,256]{1,0:T(8,128)(2,1)} %wp_ref.2, ...), custom_call_target="tpu_custom_call" | custom-call | flops 4000000000 | bytes 6000000 | tf_op jit(solution)/shard_map/gather_project/pallas_call | solution.py:277
  47.9 0.7 slice.64
  48.6 1.5 collective-permute-start
  50.2 0.6 collective-permute-done
  50.9 1.0 maximum_convert_fusion
  51.9 1.4 convolution_bitcast_fusion
  53.3 0.4 copy.22
  53.7 0.4 reshape.163
  54.2 0.0 copy-start.4
  54.2 0.0 copy-start.5
  54.2 4.4 %all_to_all.20 = bf16[2,256,256]{2,1,0:T(8,128)(2,1)S(1)} all-to-all(bf16[2,256,256]{2,1,0:T(8,128)(2,1)S(1)} %multiply_convert_fusion), channel_id=1, replica_groups=mesh['sp'=16,'fs'=4,'tp'=2] {'tp'}, dimensions={0} | all-to-all | bytes 524288 | tf_op jit(solution)/shard_map/all_to_all | solution.py:632
  58.6 7.9 %all-to-all-start.1 = ((bf16[16,192,256]{2,1,0:T(8,128)(2,1)}), bf16[16,192,256]{2,1,0:T(8,128)(2,1)S(1)}, u32[]{:S(2)}, u32[]{:S(2)}) async-start(bf16[16,192,256]{2,1,0:T(8,128)(2,1)} %get-tuple-element.12), calls=%async_computation.1 | async-start | bytes 3145728 | tf_op jit(solution)/shard_map/all_to_all | solution.py:624
  66.6 0.0 copy-done.4
  66.6 0.0 copy-done.5
  66.6 0.2 copy.23
  66.9 0.1 fusion.4
  67.0 23.6 %all-to-all-done.1.x_ref = bf16[16,192,256]{2,1,0:T(8,128)(2,1)S(1)} async-done(((bf16[16,192,256]{2,1,0:T(8,128)(2,1)}), bf16[16,192,256]{2,1,0:T(8,128)(2,1)S(1)}, u32[]{:S(2)}, u32[]{:S(2)}) %all-to-all-start.1) | async-done | bytes 1572896 | tf_op jit(solution)/shard_map/all_to_all | solution.py:624
  90.6 0.7 broadcast_in_dim.157.offset_ref
  91.3 0.6 broadcast_in_dim.158.gains_ref
  91.9 73.4 %stick_attention.1 = (bf16[16,64,256]{2,1,0:T(8,128)(2,1)}, bf16[512,2048]{1,0:T(8,128)(2,1)}, bf16[1024,2048]{1,0:T(8,128)(2,1)}, bf16[32,768]{1,0:T(8,128)(2,1)}) custom-call(f32[8,128]{1,0:T(8,128)} %broadcast_in_dim.157.offset_ref, bf16[16,192,256]{2,1,0:T(8,128)(2,1)} %copy-done.2, bf16[256,512]{1,0:T(8,128)(2,1)} %wp_ref.3, bf16[512,512]{1,0:T(8,128)(2,1)} %wa_ref.1, ...), custom_call_target="tpu_custom_call" | custom-call | flops 40000000000 | bytes 4000000 | tf_op jit(solution)/shard_map/stick_attention/pallas_call | solution.py:540
  165.3 0.7 slice_reduce_fusion.3
  166.0 3.6 %all-to-all-start.2 = ((bf16[16,64,256]{2,1,0:T(8,128)(2,1)}), bf16[16,64,256]{2,1,0:T(8,128)(2,1)S(1)}, u32[]{:S(2)}, u32[]{:S(2)}) async-start(bf16[16,64,256]{2,1,0:T(8,128)(2,1)} %get-tuple-element.15), calls=%async_computation.2 | async-start | bytes 1048576 | tf_op jit(solution)/shard_map/all_to_all | solution.py:630
  169.6 0.7 slice_reduce_fusion.1
  170.4 0.1 fusion.23
  170.5 11.2 %all-to-all-done.2 = bf16[16,64,256]{2,1,0:T(8,128)(2,1)S(1)} async-done(((bf16[16,64,256]{2,1,0:T(8,128)(2,1)}), bf16[16,64,256]{2,1,0:T(8,128)(2,1)S(1)}, u32[]{:S(2)}, u32[]{:S(2)}) %all-to-all-start.2) | async-done | bytes 524320 | tf_op jit(solution)/shard_map/all_to_all | solution.py:630
  181.7 0.2 multiply_reduce_fusion
  181.9 0.2 fusion.3
  182.1 3.6 %fusion.30 = f32[256,2048]{1,0:T(8,128)S(1)} fusion(bf16[1024,256]{1,0:T(8,128)(2,1)S(1)} %fusion.3, bf16[1024,2048]{1,0:T(8,128)(2,1)} %get-tuple-element.16), kind=kOutput, calls=%fused_computation.84 | convolution fusion | flops 1073741824 | bytes 6815744 | tf_op jit(solution)/shard_map/dot_general | solution.py:642
  185.7 1.7 fusion.1
  (26 shorter events, 0.2 us)
Async XLA Ops:
  0.0 51.9 %copy-start = (bf16[2,128,128]{2,1,0:T(8,128)(2,1)S(1)}, bf16[2,128,128]{2,1,0:T(8,128)(2,1)}, u32[]{:S(2)}) copy-start(bf16[2,128,128]{2,1,0:T(8,128)(2,1)} %param.24) | copy-start | bytes 196612
  48.6 2.3 %collective-permute-start = (bf16[16,256]{1,0:T(8,128)(2,1)S(1)}, bf16[16,256]{1,0:T(8,128)(2,1)S(1)}, u32[]{:S(2)}, u32[]{:S(2)}) collective-permute-start(bf16[16,256]{1,0:T(8,128)(2,1)S(1)} %slice.64), channel_id=1, source_target_pairs={{0,8},{8,16},{16,24},{24,32},{32,40},{40,48},{48,56},{56,64},{64,7... | collective-permute-start | bytes 24584 | tf_op jit(solution)/shard_map/ppermute | solution.py:26
  53.3 0.8 copy-start.3
  54.2 12.4 %copy-start.4 = (bf16[512]{0:T(512)(128)(2,1)S(1)}, bf16[512]{0:T(512)(128)(2,1)}, u32[]{:S(2)}) copy-start(bf16[512]{0:T(512)(128)(2,1)} %param.27) | copy-start | bytes 3076
  54.2 12.4 %copy-start.5 = (bf16[256]{0:T(256)(128)(2,1)S(1)}, bf16[256]{0:T(256)(128)(2,1)}, u32[]{:S(2)}) copy-start(bf16[256]{0:T(256)(128)(2,1)} %param.26) | copy-start | bytes 1540
  58.6 31.9 %copy-start.6 = (f32[8]{0:T(128)S(1)}, f32[8]{0:T(128)}, u32[]{:S(2)}) copy-start(f32[8]{0:T(128)} %param.23) | copy-start | bytes 100
  58.6 31.9 %all-to-all-start.1 = ((bf16[16,192,256]{2,1,0:T(8,128)(2,1)}), bf16[16,192,256]{2,1,0:T(8,128)(2,1)S(1)}, u32[]{:S(2)}, u32[]{:S(2)}) async-start(bf16[16,192,256]{2,1,0:T(8,128)(2,1)} %get-tuple-element.12), calls=%async_computation.1 | async-start | bytes 3145728 | tf_op jit(solution)/shard_map/all_to_all | solution.py:624
  90.6 1.4 copy-start.2
  166.0 15.7 %all-to-all-start.2 = ((bf16[16,64,256]{2,1,0:T(8,128)(2,1)}), bf16[16,64,256]{2,1,0:T(8,128)(2,1)S(1)}, u32[]{:S(2)}, u32[]{:S(2)}) async-start(bf16[16,64,256]{2,1,0:T(8,128)(2,1)} %get-tuple-element.15), calls=%async_computation.2 | async-start | bytes 1048576 | tf_op jit(solution)/shard_map/all_to_all | solution.py:630
  182.1 3.6 %copy-start.1 = (bf16[512,2048]{1,0:T(8,128)(2,1)S(1)}, bf16[512,2048]{1,0:T(8,128)(2,1)}, u32[]{:S(2)}) copy-start(bf16[512,2048]{1,0:T(8,128)(2,1)} %get-tuple-element.14) | copy-start | bytes 6291460

commit v3 on v2

--- a/solution.py
+++ b/solution.py
@@ -310,17 +310,30 @@
 def attention_kernel(
     offset_ref, x_ref, wp_ref, wa_ref, gains_ref,
     o_ref, wp_all, wa_all, gains_all,
-    offset_s, other_s, q_s, k_s, v_s, tri_s, acc_s, carry_s, z0, z1, l0, l1, send, recv,
+    offset_s, other_s, q_s, k_s, v_s, tri_s, mask_s, acc_s, carry_s, done_s,
+    z0, z1, z2, l0, l1, l2, w0, w1, w2, send, recv,
 ):
     sp, y, core = lax.axis_index("sp"), lax.axis_index("fs"), lax.axis_index("tp")
     y_up, y_down, y_far = (y + 1) % 4, (y + 3) % 4, (y + 2) % 4
     partner = {"sp": sp, "fs": y, "tp": 1 - core}
     up = {"sp": sp, "fs": y_up, "tp": core}
     down = {"sp": sp, "fs": y_down, "tp": core}
+
+    def owner(block):
+        return {"sp": block, "fs": y, "tp": core}
+
     barrier = pltpu.get_barrier_semaphore()
     for target in (partner, up, down):
         pl.semaphore_signal(barrier, inc=1, device_id=target, device_id_type=MESH)
-    pl.semaphore_wait(barrier, 3)
+
+    def greet(i, unused):
+        pl.semaphore_signal(
+            barrier, inc=1, device_id=owner((sp + i) % BLOCKS), device_id_type=MESH
+        )
+        return unused
+
+    lax.fori_loop(1, BLOCKS, greet, 0)
+    pl.semaphore_wait(barrier, 18)
     started = []
 
     def remote(source, target_ref, index, target):
@@ -405,25 +418,33 @@
     of_head = jnp.where(sp // 8 == core, offset_ref[pl.ds(sp % 8, 1), :], offset_s[pl.ds(sp % 8, 1), :])
     offset = of_head[:, 0:1] * math.sqrt(HEAD_DIM)
 
-    row16 = lax.broadcasted_iota(jnp.int32, (64, BLOCK), 0)
-    terms = split_terms(jnp.broadcast_to(offset, (64, BLOCK)))
+    column = lax.broadcasted_iota(jnp.int32, (BLOCK, 64), 1)
+    terms = split_terms(jnp.broadcast_to(offset, (BLOCK, 64)))
     extra = jnp.where(
-        row16 == 0,
+        column == 0,
         terms[0].astype(jnp.float32),
         jnp.where(
-            row16 == 1,
+            column == 1,
             terms[1].astype(jnp.float32),
-            jnp.where(row16 == 2, terms[2].astype(jnp.float32), 0.0),
+            jnp.where(column == 2, terms[2].astype(jnp.float32), 0.0),
         ),
     ).astype(jnp.bfloat16)
-    lane = lax.broadcasted_iota(jnp.int32, (HALF, 64), 1)
-    ones = jnp.where(lane < 3, 1.0, 0.0).astype(jnp.bfloat16)
+    row = lax.broadcasted_iota(jnp.int32, (64, HALF), 0)
+    ones = jnp.where(row < 3, 1.0, 0.0).astype(jnp.bfloat16)
     tri_s[...] = jnp.where(
         lax.broadcasted_iota(jnp.int32, (HALF, HALF), 0)
-        >= lax.broadcasted_iota(jnp.int32, (HALF, HALF), 1),
+        <= lax.broadcasted_iota(jnp.int32, (HALF, HALF), 1),
         1.0,
         0.0,
     ).astype(jnp.bfloat16)
+    mask_s[...] = jnp.where(
+        lax.broadcasted_iota(jnp.int32, (BLOCK, HALF), 0)
+        < lax.broadcasted_iota(jnp.int32, (BLOCK, HALF), 1) + half * HALF,
+        0.0,
+        -1e30,
+    )
+    acc_s[...] = jnp.zeros_like(acc_s)
+    carry_s[...] = jnp.zeros_like(carry_s)
 
     mine_at = pl.ds(pl.multiple_of(core * HALF, HALF), HALF)
     other_at = pl.ds(pl.multiple_of((1 - core) * HALF, HALF), HALF)
@@ -431,108 +452,126 @@
     def turned(block):
         return block.astype(jnp.float32).T.astype(jnp.bfloat16)
 
-    def prepare(r, unused):
-        k_s[r, 0:64, mine_at] = x_ref[r, 0:64, :]
-        k_s[r, 64:128, :] = extra
-        v_s[r, mine_at, :] = turned(x_ref[r, 64:128, :])
-        q_s[r, :, 0:64] = turned(x_ref[r, 128:192, :])
-        q_s[r, :, 64:128] = ones
+    mine_rows = pl.ds(pl.multiple_of(core * HALF, HALF), HALF)
+    other_rows = pl.ds(pl.multiple_of((1 - core) * HALF, HALF), HALF)
+
+    def prepare(n, unused):
+        for r in (2 * n, 2 * n + 1):
+            k_s[r, mine_rows, 0:64] = turned(x_ref[r, 0:64, :])
+            k_s[r, :, 64:128] = extra
+            v_s[r, :, mine_at] = x_ref[r, 64:128, :]
+            q_s[r, 0:64, :] = x_ref[r, 128:192, :]
+            q_s[r, 64:128, :] = ones
         return unused
 
-    lax.fori_loop(0, BLOCKS, prepare, 0)
+    lax.fori_loop(0, BLOCKS // 2, prepare, 0)
     got(other_s, 0)
 
-    def complete(r, unused):
-        k_s[r, 0:64, other_at] = other_s[r, 0:64, :]
-        v_s[r, other_at, :] = turned(other_s[r, 64:128, :])
+    def complete(n, unused):
+        for r in (2 * n, 2 * n + 1):
+            k_s[r, other_rows, 0:64] = turned(other_s[r, 0:64, :])
+            v_s[r, :, other_at] = other_s[r, 64:128, :]
         return unused
 
-    lax.fori_loop(0, BLOCKS, complete, 0)
-
-    def scores(r, g, z_ref, l_ref, masked):
-        z = (
-            jnp.dot(q_s[r], k_s[g], preferred_element_type=jnp.float32) * scale
-        )
-        soft = jnp.log2(1.0 + jnp.exp2(z))
-        if masked:
-            earlier = (
-                lax.broadcasted_iota(jnp.int32, (HALF, BLOCK), 1)
-                < lax.broadcasted_iota(jnp.int32, (HALF, BLOCK), 0) + half * HALF
-            )
-            soft = jnp.where(earlier, soft, 0.0)
-            z = jnp.where(earlier, z, -1e30)
-        z_ref[...] = z
-        l_ref[...] = soft.astype(jnp.bfloat16)
-
-    def weigh(r, g, z_ref, l_ref, first):
-        late = jnp.dot(l_ref[:, HALF:], tri_s[...], preferred_element_type=jnp.float32)
-        early = jnp.dot(l_ref[:, :HALF], tri_s[...], preferred_element_type=jnp.float32)
-        late_total = late[:, 0:1]
-        early_total = early[:, 0:1]
-        if first:
-            w_late = jnp.exp2(z_ref[:, HALF:] - late)
-            before = late_total
-        else:
-            carry = carry_s[r][:, 0:1]
-            w_late = jnp.exp2(z_ref[:, HALF:] - (late + carry))
-            before = carry + late_total
-        w_early = jnp.exp2(z_ref[:, :HALF] - (early + before))
-        w = jnp.concatenate([w_early.astype(jnp.bfloat16), w_late.astype(jnp.bfloat16)], axis=1)
-        out = jnp.dot(w, v_s[g], preferred_element_type=jnp.float32)
-        carry_s[r] = jnp.broadcast_to(before + early_total, (HALF, 128))
-        if first:
-            acc_s[r] = out
-        else:
-            acc_s[r] = acc_s[r] + out
-
-    scores(0, 0, z0, l0, True)
-
-    def own(n, unused):
-        r = 2 * n
-        scores(r + 1, r + 1, z1, l1, True)
-        weigh(r, r, z0, l0, True)
-        after = jnp.minimum(r + 2, BLOCKS - 1)
-        scores(after, after, z0, l0, True)
-        weigh(r + 1, r + 1, z1, l1, True)
-        return unused
-
-    lax.fori_loop(0, BLOCKS // 2, own, 0)
+    lax.fori_loop(0, BLOCKS // 2, complete, 0)
+
+    zs, ls, ws = (z0, z1, z2), (l0, l1, l2), (w0, w1, w2)
+
+    def places(state):
+        distance, r = state
+        r_in = jnp.clip(r, 0, BLOCKS - 1)
+        row_at = jnp.where((r < 0) | (r >= BLOCKS), BLOCKS, r)
+        return (row_at, r_in, jnp.clip(r_in - distance, 0, BLOCKS - 1))
 
     def advance(state):
         distance, r = state
         over = r == BLOCKS - 1
         distance = jnp.where(over, distance + 1, distance)
-        r = jnp.where(over, distance, r + 1)
-        fits = r < BLOCKS
-        return (jnp.where(fits, distance, BLOCKS - 1), jnp.where(fits, r, BLOCKS - 1))
-
-    start = (jnp.int32(1), jnp.int32(1))
-    scores(1, 0, z0, l0, False)
-
-    def earlier_blocks(n, state):
-        after = advance(state)
-        last = advance(after)
-        scores(after[1], after[1] - after[0], z1, l1, False)
-        weigh(state[1], state[1] - state[0], z0, l0, False)
-        scores(last[1], last[1] - last[0], z0, l0, False)
-        weigh(after[1], after[1] - after[0], z1, l1, False)
-        return last
-
-    state = lax.fori_loop(0, 28, earlier_blocks, start)
+        return (distance, jnp.where(over, distance, r + 1))
+
+    def scores(state, b, masked):
+        unused_row, r, g = places(state)
+        z = jnp.dot(k_s[g], q_s[r], preferred_element_type=jnp.float32) * scale
+        if masked:
+            z = z + mask_s[...]
+        zs[b][...] = z
+
+    def soften(b):
+        ls[b][...] = jnp.log2(1.0 + jnp.exp2(zs[b][...])).astype(jnp.bfloat16)
+
+    def weigh(state, b):
+        row_at = places(state)[0]
+        late = jnp.dot(tri_s[...], ls[b][HALF:, :], preferred_element_type=jnp.float32)
+        early = jnp.dot(tri_s[...], ls[b][:HALF, :], preferred_element_type=jnp.float32)
+        carry = carry_s[row_at][0:1]
+        before = carry + late[0:1]
+        ws[b][HALF:, :] = jnp.exp2(zs[b][HALF:, :] - (late + carry)).astype(jnp.bfloat16)
+        ws[b][:HALF, :] = jnp.exp2(zs[b][:HALF, :] - (early + before)).astype(jnp.bfloat16)
+        carry_s[row_at] = jnp.broadcast_to(before + early[0:1], (8, HALF))
+
+    def gather_values(state, b):
+        row_at, unused_row, g = places(state)
+        acc_s[row_at] = acc_s[row_at] + jnp.dot(
+            v_s[g], ws[b][...], preferred_element_type=jnp.float32
+        )
+
+    def steps(masked):
+        def body(n, states):
+            states = list(states)
+            for unused_step in range(6):
+                states.append(advance(states[-1]))
+            for u in range(6):
+                gather_values(states[u], (u + 2) % 3)
+                weigh(states[u + 1], u % 3)
+                soften((u + 1) % 3)
+                scores(states[u + 3], (u + 2) % 3, masked)
+            return tuple(states[6:])
+
+        return body
+
+    def return_rows(low, high):
+        def send_row(r, unused):
+            done_s[r] = acc_s[r].astype(jnp.bfloat16)
+
+            @pl.when(r != sp)
+            def _():
+                pltpu.make_async_remote_copy(
+                    src_ref=done_s.at[r], dst_ref=o_ref.at[sp], send_sem=send.at[19 + r],
+                    recv_sem=recv.at[19 + sp], device_id=owner(r), device_id_type=MESH,
+                ).start()
+
+            return unused
+
+        lax.fori_loop(low, high, send_row, 0)
+
+    first = tuple((jnp.int32(0), jnp.int32(r)) for r in (-5, -4, -3, -2))
+    states = lax.fori_loop(0, 3, steps(True), first)
+    states = lax.fori_loop(0, 8, steps(False), states)
     weights_middle()
-    state = lax.fori_loop(28, 46, earlier_blocks, state)
+    states = lax.fori_loop(8, 14, steps(False), states)
     weights_late()
-    lax.fori_loop(46, BLOCKS * (BLOCKS - 1) // 4, earlier_blocks, state)
-
-    def finish(r, unused):
-        o_ref[r] = acc_s[r].T.astype(jnp.bfloat16)
-        return unused
-
-    lax.fori_loop(0, BLOCKS, finish, 0)
+    return_rows(0, 8)
+    states = lax.fori_loop(14, 19, steps(False), states)
+    return_rows(8, 13)
+    states = lax.fori_loop(19, 21, steps(False), states)
+    return_rows(13, 16)
+    o_ref[sp] = done_s[sp]
     weights_end()
     got(gains_all.at[pl.ds(pl.multiple_of(16 * (1 - core), 16), 16), :], 1)
     for copy in started:
         copy.wait_send()
+
+    def settle_row(i, unused):
+        r = (sp + i) % BLOCKS
+        copy = pltpu.make_async_remote_copy(
+            src_ref=done_s.at[r], dst_ref=o_ref.at[r], send_sem=send.at[19 + r],
+            recv_sem=recv.at[19 + r], device_id=owner(r), device_id_type=MESH,
+        )
+        copy.wait_send()
+        copy.wait_recv()
+        return unused
+
+    lax.fori_loop(1, BLOCKS, settle_row, 0)
 
 
 def attention(offset, packed, w_pool, w_attn, gains):
@@ -550,18 +589,18 @@
         scratch_shapes=[
             pltpu.VMEM((8, 128), jnp.float32),
             pltpu.VMEM((BLOCKS, 128, HALF), jnp.bfloat16),
-            pltpu.VMEM((BLOCKS, HALF, 128), jnp.bfloat16),
-            pltpu.VMEM((BLOCKS, 128, BLOCK), jnp.bfloat16),
-            pltpu.VMEM((BLOCKS, BLOCK, HEAD_DIM), jnp.bfloat16),
+            pltpu.VMEM((BLOCKS, 128, HALF), jnp.bfloat16),
+            pltpu.VMEM((BLOCKS, BLOCK, 128), jnp.bfloat16),
+            pltpu.VMEM((BLOCKS, HEAD_DIM, BLOCK), jnp.bfloat16),
             pltpu.VMEM((HALF, HALF), jnp.bfloat16),
-            pltpu.VMEM((BLOCKS, HALF, HEAD_DIM), jnp.float32),
-            pltpu.VMEM((BLOCKS, HALF, 128), jnp.float32),
-            pltpu.VMEM((HALF, BLOCK), jnp.float32),
-            pltpu.VMEM((HALF, BLOCK), jnp.float32),
-            pltpu.VMEM((HALF, BLOCK), jnp.bfloat16),
-            pltpu.VMEM((HALF, BLOCK), jnp.bfloat16),
-            pltpu.SemaphoreType.DMA((19,)),
-            pltpu.SemaphoreType.DMA((19,)),
+            pltpu.VMEM((BLOCK, HALF), jnp.float32),
+            pltpu.VMEM((BLOCKS + 1, HEAD_DIM, HALF), jnp.float32),
+            pltpu.VMEM((BLOCKS + 1, 8, HALF), jnp.float32),
+            pltpu.VMEM((BLOCKS, HEAD_DIM, HALF), jnp.bfloat16),
+            *[pltpu.VMEM((BLOCK, HALF), jnp.float32)] * 3,
+            *[pltpu.VMEM((BLOCK, HALF), jnp.bfloat16)] * 6,
+            pltpu.SemaphoreType.DMA((35,)),
+            pltpu.SemaphoreType.DMA((35,)),
         ],
         compiler_params=pltpu.CompilerParams(
             collective_id=1, has_side_effects=True, vmem_limit_bytes=56 * 1024 * 1024
@@ -627,7 +666,7 @@
     attended, w_pool_all, w_attn_all, gains_all = attention(
         offset, packed, w_out_pool, w_out_attn, gains
     )
-    attended = lax.all_to_all(attended, "sp", 0, 0, tiled=True).reshape(HEADS * HEAD_DIM, HALF)
+    attended = attended.reshape(HEADS * HEAD_DIM, HALF)
     pool_out = pooling(pool_in, pool_mix, pool_scale)
     pool_rows = lax.all_to_all(pool_out, "tp", split_axis=0, concat_axis=1, tiled=True)
     pool_gain_all = jnp.concatenate([gains_all[0, :256], gains_all[16, :256]])

time: 188 us -> 163 us (0.87); the launches traced: 187 us -> 160 us
  Pallas kernels: 119 us -> 103 us
  waiting for transfers between devices: 35.4 us -> 24.2 us
  starting transfers between devices: 13 us -> 9.4 us
  other arithmetic: 1.84 us -> 3.92 us
    pallas_call x1, Pallas kernels: 73.4 us -> 58.1 us  [attention(): pl.pallas_call(attention_kernel, out_shape=(jax.ShapeDtypeStruct((BLOCKS,...]
    all_to_all x1 -> x0, waiting for transfers between devices: 11.2 us -> none  [shards(): lax.all_to_all(attended, 'sp', 0, 0, tiled=True)]
    all_to_all x1 -> x0, starting transfers between devices: 3.58 us -> none  [shards(): lax.all_to_all(attended, 'sp', 0, 0, tiled=True)]
  transfers between devices with their start and end apart: 3 -> 2, of which waited for: 3 -> 2; matrix products, arithmetic and copies ran while one was open for 1% -> 0% of each run, Pallas kernels for 0% -> 0%
where the time goes in v3:
time: 163 us; the launch traced here: 160 us
  Pallas kernels  103 us (63%)
  waiting for transfers between devices  24.2 us (15%)
  starting transfers between devices  9.4 us (6%)
  local copies, waits for them, and re-layouts  7.35 us (5%)
  matrix products  6.74 us (4%)
  blocking collectives  4.42 us (3%)
  other arithmetic  3.92 us (2%)
    pallas_call x1, Pallas kernels, attention(): pl.pallas_call(attention_kernel, out_shape=(jax.ShapeDtypeStruct((BLOCKS,...  58.1 us
    pallas_call x1, Pallas kernels, project(): pl.pallas_call(project_kernel, out_shape=(jax.ShapeDtypeStruct((HEADS, 3...  45.1 us
    all_to_all x1, waiting for transfers between devices, shards(): packed = lax.all_to_all(packed, 'sp', 0, 0, tiled=True)  23.6 us
    all_to_all x1, starting transfers between devices, shards(): packed = lax.all_to_all(packed, 'sp', 0, 0, tiled=True)  7.91 us
    all_to_all x1, blocking collectives, shards(): lax.all_to_all(pool_out, 'tp', split_axis=0, concat_axis=1, tiled=True)  4.42 us
    dot_general x1, matrix products, shards(): lax.dot_general(attn_normed, w_attn_all, (((0,), (0,)), ((), ())), prefer...  3.61 us
  transfers between devices with their start and end apart: 2, of which 2 were waited for; matrix products, arithmetic and copies ran while one was open for 0% of the time, Pallas kernels for 0%

profile of v3, /device:TPU:1, one launch (start us, length us, event | category | flops | bytes accessed | tf_op | source)
XLA Modules:
  0.0 159.5 jit_solution(9411973230796854895)
XLA Ops:
  0.0 0.0 copy-start
  0.0 1.4 copy.20.qg_ref
  1.4 1.4 copy.19.kg_ref
  2.8 45.1 %gather_project.1 = (bf16[16,192,256]{2,1,0:T(8,128)(2,1)}, bf16[512,256]{1,0:T(8,128)(2,1)}) custom-call(bf16[512,1024]{1,0:T(8,128)(2,1)} %bitcast.36, f32[4,1,512]{2,1,0:T(1,128)} %bitcast.37, bf16[512,512]{1,0:T(8,128)(2,1)} %wk_ref.1, bf16[512,512]{1,0:T(8,128)(2,1)} %wv_ref.1, bf16[512,512]{1,0:T(8,128)(2,1)} %wq_ref.1, bf16[512,256]{1,0:T(8,128)(2,1)} %wp_ref.2, ...), custom_call_target="tpu_custom_call" | custom-call | flops 4000000000 | bytes 6000000 | tf_op jit(solution)/shard_map/gather_project/pallas_call | solution.py:277
  47.9 0.7 slice.64
  48.6 1.5 collective-permute-start
  50.3 0.6 collective-permute-done
  50.9 1.0 maximum_convert_fusion
  51.9 0.0 copy-done
  51.9 1.4 convolution_bitcast_fusion
  53.3 0.4 copy.22
  53.7 0.4 reshape.163
  54.2 0.0 copy-done.3
  54.2 0.0 copy-start.4
  54.2 0.0 copy-start.5
  54.2 4.4 %all_to_all.15 = bf16[2,256,256]{2,1,0:T(8,128)(2,1)S(1)} all-to-all(bf16[2,256,256]{2,1,0:T(8,128)(2,1)S(1)} %multiply_convert_fusion), channel_id=1, replica_groups=mesh['sp'=16,'fs'=4,'tp'=2] {'tp'}, dimensions={0} | all-to-all | bytes 524288 | tf_op jit(solution)/shard_map/all_to_all | solution.py:671
  58.7 7.9 %all-to-all-start.1 = ((bf16[16,192,256]{2,1,0:T(8,128)(2,1)}), bf16[16,192,256]{2,1,0:T(8,128)(2,1)S(1)}, u32[]{:S(2)}, u32[]{:S(2)}) async-start(bf16[16,192,256]{2,1,0:T(8,128)(2,1)} %get-tuple-element.12), calls=%async_computation.1 | async-start | bytes 3145728 | tf_op jit(solution)/shard_map/all_to_all | solution.py:663
  66.6 0.0 copy-done.4
  66.7 0.2 copy.23
  66.9 0.1 fusion.4
  67.0 23.6 %all-to-all-done.1.x_ref = bf16[16,192,256]{2,1,0:T(8,128)(2,1)S(1)} async-done(((bf16[16,192,256]{2,1,0:T(8,128)(2,1)}), bf16[16,192,256]{2,1,0:T(8,128)(2,1)S(1)}, u32[]{:S(2)}, u32[]{:S(2)}) %all-to-all-start.1) | async-done | bytes 1572896 | tf_op jit(solution)/shard_map/all_to_all | solution.py:663
  90.6 0.8 broadcast_in_dim.157.offset_ref
  91.4 0.6 broadcast_in_dim.158.gains_ref
  92.0 58.1 %stick_attention.1 = (bf16[16,64,256]{2,1,0:T(8,128)(2,1)}, bf16[512,2048]{1,0:T(8,128)(2,1)}, bf16[1024,2048]{1,0:T(8,128)(2,1)}, bf16[32,768]{1,0:T(8,128)(2,1)}) custom-call(f32[8,128]{1,0:T(8,128)} %broadcast_in_dim.157.offset_ref, bf16[16,192,256]{2,1,0:T(8,128)(2,1)} %copy-done.2, bf16[256,512]{1,0:T(8,128)(2,1)} %wp_ref.3, bf16[512,512]{1,0:T(8,128)(2,1)} %wa_ref.1, ...), custom_call_target="tpu_custom_call" | custom-call | flops 40000000000 | bytes 4000000 | tf_op jit(solution)/shard_map/stick_attention/pallas_call | solution.py:579
  150.1 0.7 slice_reduce_fusion.3
  150.8 0.7 slice_reduce_fusion.1
  151.6 1.2 multiply_reduce_fusion
  152.8 1.2 fusion.3
  154.1 3.6 %fusion.30 = f32[256,2048]{1,0:T(8,128)S(1)} fusion(bf16[1024,256]{1,0:T(8,128)(2,1)S(1)} %fusion.3, bf16[1024,2048]{1,0:T(8,128)(2,1)} %get-tuple-element.16), kind=kOutput, calls=%fused_computation.84 | convolution fusion | flops 1073741824 | bytes 6815744 | tf_op jit(solution)/shard_map/dot_general | solution.py:681
  157.7 0.1 fusion.23
  157.8 0.0 copy-done.1
  157.8 1.7 %fusion.1 = bf16[1,256,2048]{2,1,0:T(8,128)(2,1)} fusion(f32[256,2048]{1,0:T(8,128)S(1)} %fusion.30, bf16[256,512]{0,1:T(8,128)(2,1)S(1)} %fusion.23, bf16[512,2048]{1,0:T(8,128)(2,1)S(1)} %copy-done.1), kind=kOutput, calls=%fused_computation.2 | convolution fusion | flops 537919488 | bytes 5505024 | tf_op jit(solution)/shard_map/dot_general | solution.py:681
  (24 shorter events, 0.2 us)
Async XLA Ops:
  0.0 51.9 %copy-start = (bf16[2,128,128]{2,1,0:T(8,128)(2,1)S(1)}, bf16[2,128,128]{2,1,0:T(8,128)(2,1)}, u32[]{:S(2)}) copy-start(bf16[2,128,128]{2,1,0:T(8,128)(2,1)} %param.24) | copy-start | bytes 196612
  48.6 2.3 %collective-permute-start = (bf16[16,256]{1,0:T(8,128)(2,1)S(1)}, bf16[16,256]{1,0:T(8,128)(2,1)S(1)}, u32[]{:S(2)}, u32[]{:S(2)}) collective-permute-start(bf16[16,256]{1,0:T(8,128)(2,1)S(1)} %slice.64), channel_id=1, source_target_pairs={{0,8},{8,16},{16,24},{24,32},{32,40},{40,48},{48,56},{56,64},{64,7... | collective-permute-start | bytes 24584 | tf_op jit(solution)/shard_map/ppermute | solution.py:26
  53.3 0.8 copy-start.3
  54.2 12.4 %copy-start.4 = (bf16[512]{0:T(512)(128)(2,1)S(1)}, bf16[512]{0:T(512)(128)(2,1)}, u32[]{:S(2)}) copy-start(bf16[512]{0:T(512)(128)(2,1)} %param.27) | copy-start | bytes 3076
  54.2 12.4 %copy-start.5 = (bf16[256]{0:T(256)(128)(2,1)S(1)}, bf16[256]{0:T(256)(128)(2,1)}, u32[]{:S(2)}) copy-start(bf16[256]{0:T(256)(128)(2,1)} %param.26) | copy-start | bytes 1540
  58.7 31.9 %copy-start.6 = (f32[8]{0:T(128)S(1)}, f32[8]{0:T(128)}, u32[]{:S(2)}) copy-start(f32[8]{0:T(128)} %param.23) | copy-start | bytes 100
  58.7 31.9 %all-to-all-start.1 = ((bf16[16,192,256]{2,1,0:T(8,128)(2,1)}), bf16[16,192,256]{2,1,0:T(8,128)(2,1)S(1)}, u32[]{:S(2)}, u32[]{:S(2)}) async-start(bf16[16,192,256]{2,1,0:T(8,128)(2,1)} %get-tuple-element.12), calls=%async_computation.1 | async-start | bytes 3145728 | tf_op jit(solution)/shard_map/all_to_all | solution.py:663
  90.6 1.4 copy-start.2
  154.0 3.8 %copy-start.1 = (bf16[512,2048]{1,0:T(8,128)(2,1)S(1)}, bf16[512,2048]{1,0:T(8,128)(2,1)}, u32[]{:S(2)}) copy-start(bf16[512,2048]{1,0:T(8,128)(2,1)} %get-tuple-element.14) | copy-start | bytes 6291460

commit v4 on v3

--- a/solution.py
+++ b/solution.py
@@ -1,4 +1,3 @@
-import functools
 import math
 
 import jax
@@ -20,12 +19,6 @@
 LOG2E = 1.4426950408889634
 
 
-def shifted_2(value, axis, steps):
-    count = lax.axis_size(axis)
-    initial, last = (max(0, -steps), min(count, count - steps))
-    return lax.ppermute(value, axis, [(source, source + steps) for source in range(initial, last)])
-
-
 def branch_norm(values_in, squares, width, gain):
     values_f = values_in.astype(jnp.float32)
     factor = lax.rsqrt(squares / width + EPS)
@@ -44,9 +37,9 @@
 
 
 def project_kernel(
-    tok_ref, gain_ref, wk_ref, wv_ref, wq_ref, wp_ref, kg_ref, qg_ref,
+    tok_ref, gain_ref, wk_ref, wv_ref, wq_ref, wp_ref, kg_ref, qg_ref, mix_ref, scale_ref,
     out_ref, pool_ref,
-    buf, pbuf, tok_s, x_s, acc, acc_p, mine, theirs, send, recv,
+    buf, pbuf, tok_s, x_s, acc, acc_p, heads_s, pool_in, before_s, pooled_s, send, recv,
 ):
     sp, y, core = lax.axis_index("sp"), lax.axis_index("fs"), lax.axis_index("tp")
     z, x = sp // 4, sp % 4
@@ -65,9 +58,19 @@
     }
 
     barrier = pltpu.get_barrier_semaphore()
-    for target in (partner, *to.values()):
+    for target in (partner, to["yp"], to["ym"]):
         pl.semaphore_signal(barrier, inc=1, device_id=target, device_id_type=MESH)
-    pl.semaphore_wait(barrier, 7)
+
+    def greet(i, unused):
+        for of_core in range(2):
+            pl.semaphore_signal(
+                barrier, inc=1, device_id={"sp": (sp + i) % BLOCKS, "fs": y, "tp": of_core},
+                device_id_type=MESH,
+            )
+        return unused
+
+    lax.fori_loop(1, BLOCKS, greet, 0)
+    pl.semaphore_wait(barrier, 33)
 
     started = []
 
@@ -196,23 +199,54 @@
             total = total + jnp.dot(x_s[q], buf[a, q], preferred_element_type=jnp.float32)
         return total
 
+    def head_copy(a, i, source):
+        h, of_core = (sp + i // 2) % 8, i % 2
+        return pltpu.make_async_remote_copy(
+            src_ref=heads_s.at[a, h, of_core],
+            dst_ref=out_ref.at[source, a * 64 : a * 64 + 64, :],
+            send_sem=send.at[97 + a * 16 + i], recv_sem=recv.at[97 + a * 16 + source],
+            device_id={"sp": 8 * core + h, "fs": y, "tp": of_core}, device_id_type=MESH,
+        )
+
+    stays = sp // 8 == core
+
     def deliver(a, total):
         turned = total.T.reshape(8, HEAD_DIM, BLOCK)
         if a != 1:
             factor = lax.rsqrt(jnp.mean(turned * turned, axis=1, keepdims=True) + EPS)
-            gain = (kg_ref if a == 0 else qg_ref)[...]
+            gain_row = (kg_ref if a == 0 else qg_ref)[...]
+            gain = jnp.broadcast_to(gain_row, (HEAD_DIM, HEAD_DIM)).T[:, 0:1]
             turned = turned * factor * gain[None]
         turned = turned.astype(jnp.bfloat16)
-        is_first = core == 0
-        low, high = turned[:, :, :HALF], turned[:, :, HALF:]
-        out_ref[pl.ds(8 * core, 8), a * 64 : a * 64 + 64, :] = jnp.where(is_first, low, high)
-        theirs[a] = jnp.where(is_first, high, low)
-        go(
-            theirs.at[a],
-            out_ref.at[pl.ds(8 * core, 8), a * 64 : a * 64 + 64, :],
-            95 + a,
-            partner,
-        )
+        heads_s[a, :, 0] = turned[:, :, :HALF]
+        heads_s[a, :, 1] = turned[:, :, HALF:]
+
+        def send_head(i, unused):
+            @pl.when(jnp.logical_not(stays & (i == core)))
+            def _():
+                head_copy(a, i, sp).start()
+
+            return unused
+
+        lax.fori_loop(0, 16, send_head, 0)
+
+        @pl.when(stays)
+        def _():
+            out_ref[sp, a * 64 : a * 64 + 64, :] = heads_s[a, sp % 8, core]
+
+    def delivered(a):
+        def wait_head(i, unused):
+            @pl.when(jnp.logical_not(stays & (i == core)))
+            def _():
+                head_copy(a, i, sp).wait_send()
+
+            @pl.when(jnp.logical_not(stays & (i == sp)))
+            def _():
+                head_copy(a, 0, i).wait_recv()
+
+            return unused
+
+        lax.fori_loop(0, 16, wait_head, 0)
 
     go(tok_ref, tok_s, 94, partner)
     direct(0)
@@ -265,22 +299,51 @@
     total = acc_p[...]
     for q in quarters:
         total = total + jnp.dot(x_s[q], pbuf[q], preferred_element_type=jnp.float32)
-    pool_ref[...] = total.astype(jnp.bfloat16)
+    pool_in[...] = total.astype(jnp.bfloat16)
+    tail = pool_in.at[BLOCK - 16 : BLOCK, :]
+    go(tail, before_s, 95, {"sp": (sp + 1) % BLOCKS, "fs": y, "tp": core})
+    current = pool_in[...].astype(jnp.float32)
+    got(before_s, 95)
+    before = jnp.where(sp == 0, 0.0, before_s[...].astype(jnp.float32))
+
+    def behind(values, count):
+        return jnp.concatenate([jnp.zeros((count, values.shape[1]), jnp.float32), values[:-count]], axis=0)
+
+    extended = jnp.concatenate([before, current], axis=0)
+    sum_2 = extended + behind(extended, 1)
+    sum_4 = sum_2 + behind(sum_2, 2)
+    sum_8 = sum_4 + behind(sum_4, 4)
+    sum_16 = sum_8 + behind(sum_8, 8)
+    position = lax.broadcasted_iota(jnp.int32, (BLOCK, 128), 0) + (sp * BLOCK + 1)
+    for group in range(2):
+        columns = slice(128 * group, 128 * group + 128)
+        low, high = ((sum_2, sum_8), (sum_4, sum_16))[group]
+        window = jnp.where(core == 0, 2 << group, 8 << group)
+        summed = jnp.where(core == 0, low[16:, columns], high[16:, columns])
+        counted = jnp.minimum(position, window).astype(jnp.float32)
+        centered = (summed / counted - current[:, columns]).astype(jnp.bfloat16)
+        mixed = jnp.dot(centered, mix_ref[group], preferred_element_type=jnp.float32)
+        pooled_s[:, columns] = (mixed * scale_ref[:, columns]).astype(jnp.bfloat16)
+    mine_rows = pl.ds(pl.multiple_of(core * HALF, HALF), HALF)
+    other_rows = pl.ds(pl.multiple_of((1 - core) * HALF, HALF), HALF)
+    go(pooled_s.at[other_rows, :], pool_ref.at[core], 96, partner)
+    pool_ref[core] = pooled_s[mine_rows, :]
+    got(pool_ref.at[1 - core], 96)
     for a in range(3):
-        got(out_ref.at[pl.ds(8 * (1 - core), 8), a * 64 : a * 64 + 64, :], 95 + a)
+        delivered(a)
     for copy in started:
         copy.wait_send()
 
 
-def project(tokens, norm_gain, wk, wv, wq, wp, key_gain, query_gain):
+def project(tokens, norm_gain, wk, wv, wq, wp, key_gain, query_gain, pool_mix, pool_scale):
     vmem = pl.BlockSpec(memory_space=pltpu.VMEM)
     return pl.pallas_call(
         project_kernel,
         out_shape=(
             jax.ShapeDtypeStruct((HEADS, 3 * HEAD_DIM, HALF), jnp.bfloat16),
-            jax.ShapeDtypeStruct((BLOCK, 256), jnp.bfloat16),
+            jax.ShapeDtypeStruct((2, HALF, 256), jnp.bfloat16),
         ),
-        in_specs=[vmem] * 8,
+        in_specs=[vmem] * 10,
         out_specs=(vmem, vmem),
         scratch_shapes=[
             pltpu.VMEM((3, 4, 512, 512), jnp.bfloat16),
@@ -289,10 +352,12 @@
             pltpu.VMEM((4, 512, 512), jnp.bfloat16),
             pltpu.VMEM((3, 512, 512), jnp.float32),
             pltpu.VMEM((512, 256), jnp.float32),
-            pltpu.VMEM((8, 128), jnp.float32),
-            pltpu.VMEM((3, 8, HEAD_DIM, HALF), jnp.bfloat16),
-            pltpu.SemaphoreType.DMA((98,)),
-            pltpu.SemaphoreType.DMA((98,)),
+            pltpu.VMEM((3, 8, 2, HEAD_DIM, HALF), jnp.bfloat16),
+            pltpu.VMEM((512, 256), jnp.bfloat16),
+            pltpu.VMEM((16, 256), jnp.bfloat16),
+            pltpu.VMEM((512, 256), jnp.bfloat16),
+            pltpu.SemaphoreType.DMA((145,)),
+            pltpu.SemaphoreType.DMA((145,)),
         ],
         compiler_params=pltpu.CompilerParams(
             collective_id=0, has_side_effects=True, vmem_limit_bytes=56 * 1024 * 1024
@@ -303,14 +368,15 @@
         name="gather_project",
     )(
         tokens, norm_gain.reshape(4, 1, 512), wk, wv, wq, wp,
-        key_gain.reshape(HEAD_DIM, 1), query_gain.reshape(HEAD_DIM, 1),
+        key_gain.reshape(1, HEAD_DIM), query_gain.reshape(1, HEAD_DIM), pool_mix,
+        pool_scale.reshape(1, 256),
     )
 
 
 def attention_kernel(
-    offset_ref, x_ref, wp_ref, wa_ref, gains_ref,
+    offset_ref, x_ref, wp_ref, wa_ref, pg_ref, ag_ref,
     o_ref, wp_all, wa_all, gains_all,
-    offset_s, other_s, q_s, k_s, v_s, tri_s, mask_s, acc_s, carry_s, done_s,
+    offset_s, offset_m, gains_m, other_s, q_s, k_s, v_s, tri_s, mask_s, acc_s, carry_s, done_s,
     z0, z1, z2, l0, l1, l2, w0, w1, w2, send, recv,
 ):
     sp, y, core = lax.axis_index("sp"), lax.axis_index("fs"), lax.axis_index("tp")
@@ -403,20 +469,25 @@
         shared(y_up, 14)
         shared(y_far, 16)
 
-    go(offset_ref, offset_s, 18, partner)
+    offset_m[...] = jnp.zeros_like(offset_m)
+    offset_m[:, 0:8] = jnp.broadcast_to(offset_ref[...], (8, 8))
+    gains_m[:, 0:256] = jnp.broadcast_to(pg_ref[...], (16, 256))
+    gains_m[:, 256:768] = jnp.broadcast_to(ag_ref[...], (16, 512))
     keys_values = x_ref.at[:, 0:128, :]
     go(keys_values, other_s, 0, partner)
-    go(gains_ref, gains_all.at[pl.ds(pl.multiple_of(16 * core, 16), 16), :], 1, partner)
     weights_start()
+    go(offset_m, offset_s, 18, partner)
+    go(gains_m, gains_all.at[pl.ds(pl.multiple_of(16 * core, 16), 16), :], 1, partner)
     wa_part(y, core, 0, 512)[...] = wa_ref[...]
     wp_part(y, core, 0, 256)[...] = wp_ref[...]
-    gains_all[pl.ds(pl.multiple_of(16 * core, 16), 16), :] = gains_ref[...]
+    gains_all[pl.ds(pl.multiple_of(16 * core, 16), 16), :] = gains_m[...]
 
     scale = LOG2E / math.sqrt(HEAD_DIM)
     half = core
     got(offset_s, 18)
-    of_head = jnp.where(sp // 8 == core, offset_ref[pl.ds(sp % 8, 1), :], offset_s[pl.ds(sp % 8, 1), :])
-    offset = of_head[:, 0:1] * math.sqrt(HEAD_DIM)
+    of_core = jnp.where(sp // 8 == core, offset_m[0:1, :], offset_s[0:1, :])
+    chosen = lax.broadcasted_iota(jnp.int32, (1, 128), 1) == sp % 8
+    offset = jnp.sum(jnp.where(chosen, of_core, 0.0), axis=1, keepdims=True) * math.sqrt(HEAD_DIM)
 
     column = lax.broadcasted_iota(jnp.int32, (BLOCK, 64), 1)
     terms = split_terms(jnp.broadcast_to(offset, (BLOCK, 64)))
@@ -477,17 +548,26 @@
 
     zs, ls, ws = (z0, z1, z2), (l0, l1, l2), (w0, w1, w2)
 
+    first_row = jnp.where(sp == BLOCKS - 1, 1, sp + 1)
+
     def places(state):
-        distance, r = state
-        r_in = jnp.clip(r, 0, BLOCKS - 1)
-        row_at = jnp.where((r < 0) | (r >= BLOCKS), BLOCKS, r)
-        return (row_at, r_in, jnp.clip(r_in - distance, 0, BLOCKS - 1))
+        step, r, distance = state
+        row_at = jnp.where((step < 0) | (step >= 136), BLOCKS, r)
+        return (row_at, r, jnp.maximum(r - distance, 0))
 
     def advance(state):
-        distance, r = state
-        over = r == BLOCKS - 1
-        distance = jnp.where(over, distance + 1, distance)
-        return (distance, jnp.where(over, distance, r + 1))
+        step, r, distance = state
+        diagonal = step < BLOCKS - 1
+        turn = step == BLOCKS - 1
+        done = distance >= r
+        next_row = jnp.where(r == BLOCKS - 1, 1, r + 1)
+        r_after = jnp.where(
+            diagonal,
+            jnp.maximum(step + 1, 0),
+            jnp.where(turn, first_row, jnp.where(done, next_row, r)),
+        )
+        after = jnp.where(diagonal, 0, jnp.where(turn | done, 1, distance + 1))
+        return (step + 1, r_after, after)
 
     def scores(state, b, masked):
         unused_row, r, g = places(state)
@@ -514,6 +594,20 @@
         acc_s[row_at] = acc_s[row_at] + jnp.dot(
             v_s[g], ws[b][...], preferred_element_type=jnp.float32
         )
+
+    def return_row(state):
+        step, r, distance = state
+
+        @pl.when((distance == r) & (step >= 0) & (step < 136))
+        def _():
+            done_s[r] = acc_s[r].astype(jnp.bfloat16)
+
+            @pl.when(r != sp)
+            def _():
+                pltpu.make_async_remote_copy(
+                    src_ref=done_s.at[r], dst_ref=o_ref.at[sp], send_sem=send.at[19 + r],
+                    recv_sem=recv.at[19 + sp], device_id=owner(r), device_id_type=MESH,
+                ).start()
 
     def steps(masked):
         def body(n, states):
@@ -525,36 +619,19 @@
                 weigh(states[u + 1], u % 3)
                 soften((u + 1) % 3)
                 scores(states[u + 3], (u + 2) % 3, masked)
+            for u in range(6):
+                return_row(states[u])
             return tuple(states[6:])
 
         return body
 
-    def return_rows(low, high):
-        def send_row(r, unused):
-            done_s[r] = acc_s[r].astype(jnp.bfloat16)
-
-            @pl.when(r != sp)
-            def _():
-                pltpu.make_async_remote_copy(
-                    src_ref=done_s.at[r], dst_ref=o_ref.at[sp], send_sem=send.at[19 + r],
-                    recv_sem=recv.at[19 + sp], device_id=owner(r), device_id_type=MESH,
-                ).start()
-
-            return unused
-
-        lax.fori_loop(low, high, send_row, 0)
-
-    first = tuple((jnp.int32(0), jnp.int32(r)) for r in (-5, -4, -3, -2))
+    first = tuple((jnp.int32(step), jnp.int32(0), jnp.int32(0)) for step in (-5, -4, -3, -2))
     states = lax.fori_loop(0, 3, steps(True), first)
     states = lax.fori_loop(0, 8, steps(False), states)
     weights_middle()
     states = lax.fori_loop(8, 14, steps(False), states)
     weights_late()
-    return_rows(0, 8)
-    states = lax.fori_loop(14, 19, steps(False), states)
-    return_rows(8, 13)
-    states = lax.fori_loop(19, 21, steps(False), states)
-    return_rows(13, 16)
+    lax.fori_loop(14, 21, steps(False), states)
     o_ref[sp] = done_s[sp]
     weights_end()
     got(gains_all.at[pl.ds(pl.multiple_of(16 * (1 - core), 16), 16), :], 1)
@@ -574,7 +651,7 @@
     lax.fori_loop(1, BLOCKS, settle_row, 0)
 
 
-def attention(offset, packed, w_pool, w_attn, gains):
+def attention(offset, packed, w_pool, w_attn, pool_gain, attn_gain):
     vmem = pl.BlockSpec(memory_space=pltpu.VMEM)
     return pl.pallas_call(
         attention_kernel,
@@ -584,10 +661,12 @@
             jax.ShapeDtypeStruct((1024, 2048), jnp.bfloat16),
             jax.ShapeDtypeStruct((32, 768), jnp.bfloat16),
         ),
-        in_specs=[vmem] * 5,
+        in_specs=[vmem] * 6,
         out_specs=(vmem, vmem, vmem, vmem),
         scratch_shapes=[
             pltpu.VMEM((8, 128), jnp.float32),
+            pltpu.VMEM((8, 128), jnp.float32),
+            pltpu.VMEM((16, 768), jnp.bfloat16),
             pltpu.VMEM((BLOCKS, 128, HALF), jnp.bfloat16),
             pltpu.VMEM((BLOCKS, 128, HALF), jnp.bfloat16),
             pltpu.VMEM((BLOCKS, BLOCK, 128), jnp.bfloat16),
@@ -609,35 +688,7 @@
             flops=40_000_000_000, bytes_accessed=4_000_000, transcendentals=50_000_000
         ),
         name="stick_attention",
-    )(offset, packed, w_pool, w_attn, gains)
-
-
-def pooling(pool_in, pool_mix, pool_scale):
-    row_count, pool_cols = pool_in.shape
-    reach = 16
-    previous = shifted_2(pool_in[row_count - reach :], "sp", 1)
-    extended = jnp.concatenate([previous, pool_in], axis=0).astype(jnp.float32)
-    group_ch = POOL // POOL_GROUPS
-    local_groups = pool_cols // group_ch
-    group_ids = (
-        lax.axis_index("tp") * local_groups + jnp.arange(pool_cols, dtype=jnp.int32) // group_ch
-    )
-    window = jnp.left_shift(jnp.int32(2), group_ids)
-    summed = jnp.zeros((row_count, pool_cols), jnp.float32)
-    for behind in range(reach):
-        shifted = extended[reach - behind : reach - behind + row_count]
-        summed = summed + jnp.where(behind < window[None, :], shifted, 0.0)
-    sp_index = lax.axis_index("sp")
-    position = sp_index * row_count + jnp.arange(row_count, dtype=jnp.int32)
-    counted = jnp.minimum(position[:, None] + 1, window[None, :]).astype(jnp.float32)
-    centered = (summed / counted - extended[reach:]).astype(jnp.bfloat16)
-    pooled = jnp.einsum(
-        "tgc,gcd->tgd",
-        centered.reshape(row_count, local_groups, group_ch),
-        pool_mix,
-        preferred_element_type=jnp.float32,
-    )
-    return (pooled.reshape(row_count, pool_cols) * pool_scale).astype(jnp.bfloat16)
+    )(offset, packed, w_pool, w_attn, pool_gain, attn_gain)
 
 
 def shards(
@@ -657,18 +708,16 @@
     w_out_pool,
     w_out_attn,
 ):
-    packed, pool_in = project(
-        tokens[0], norm_gain, w_key, w_value, w_query, w_pool_in, key_gain, query_gain
+    packed, pool_parts = project(
+        tokens[0], norm_gain, w_key, w_value, w_query, w_pool_in, key_gain, query_gain,
+        pool_mix, pool_scale,
     )
-    packed = lax.all_to_all(packed, "sp", 0, 0, tiled=True)
-    offset = jnp.broadcast_to(stick_offset[:, None], (8, 128))
-    gains = jnp.broadcast_to(jnp.concatenate([pool_gain, attn_gain])[None], (16, 768))
     attended, w_pool_all, w_attn_all, gains_all = attention(
-        offset, packed, w_out_pool, w_out_attn, gains
+        stick_offset.reshape(1, 8), packed, w_out_pool, w_out_attn,
+        pool_gain.reshape(1, 256), attn_gain.reshape(1, 512),
     )
     attended = attended.reshape(HEADS * HEAD_DIM, HALF)
-    pool_out = pooling(pool_in, pool_mix, pool_scale)
-    pool_rows = lax.all_to_all(pool_out, "tp", split_axis=0, concat_axis=1, tiled=True)
+    pool_rows = jnp.concatenate([pool_parts[0], pool_parts[1]], axis=1)
     pool_gain_all = jnp.concatenate([gains_all[0, :256], gains_all[16, :256]])
     attn_gain_all = jnp.concatenate([gains_all[0, 256:], gains_all[16, 256:]])
     pool_f = pool_rows.astype(jnp.float32)

time: 163 us -> 143 us (0.88); the launches traced: 160 us -> 142 us
  Pallas kernels: 103 us -> 129 us
  waiting for transfers between devices: 24.2 us -> 0 us
  starting transfers between devices: 9.4 us -> 0 us
  blocking collectives: 4.42 us -> 0 us
  local copies, waits for them, and re-layouts: 7.35 us -> 4.86 us
    pallas_call x1, Pallas kernels: 45.1 us -> 69.1 us  [project(): pl.pallas_call(project_kernel, out_shape=(jax.ShapeDtypeStruct((HEADS, 3...]
    all_to_all x1 -> x0, waiting for transfers between devices: 23.6 us -> none  [shards(): packed = lax.all_to_all(packed, 'sp', 0, 0, tiled=True)]
    all_to_all x1 -> x0, starting transfers between devices: 7.91 us -> none  [shards(): packed = lax.all_to_all(packed, 'sp', 0, 0, tiled=True)]
    all_to_all x1 -> x0, blocking collectives: 4.42 us -> none  [shards(): lax.all_to_all(pool_out, 'tp', split_axis=0, concat_axis=1, tiled=True)]
  transfers between devices with their start and end apart: 2 -> 0, of which waited for: 2 -> 0; matrix products, arithmetic and copies ran while one was open for 0% -> 0% of each run, Pallas kernels for 0% -> 0%
where the time goes in v4:
time: 143 us; the launch traced here: 142 us
  Pallas kernels  129 us (90%)
  matrix products  5.35 us (4%)
  local copies, waits for them, and re-layouts  4.86 us (3%)
  other arithmetic  2.62 us (2%)
    pallas_call x1, Pallas kernels, project(): pl.pallas_call(project_kernel, out_shape=(jax.ShapeDtypeStruct((HEADS, 3...  69.1 us
    pallas_call x1, Pallas kernels, attention(): pl.pallas_call(attention_kernel, out_shape=(jax.ShapeDtypeStruct((BLOCKS,...  59.7 us
    dot_general x1, matrix products, shards(): lax.dot_general(attn_normed, w_attn_all, (((0,), (0,)), ((), ())), prefer...  3.61 us

profile of v4, /device:TPU:1, one launch (start us, length us, event | category | flops | bytes accessed | tf_op | source)
XLA Modules:
  0.0 141.7 jit_solution(3989206780873208281)
XLA Ops:
  0.0 1.2 reshape.71.pg_ref
  1.2 1.3 reshape.72.ag_ref
  2.4 69.1 %gather_project.1 = (bf16[16,192,256]{2,1,0:T(8,128)(2,1)}, bf16[2,256,256]{2,1,0:T(8,128)(2,1)}) custom-call(bf16[512,1024]{1,0:T(8,128)(2,1)} %bitcast.21, f32[4,1,512]{2,1,0:T(1,128)} %bitcast.22, bf16[512,512]{1,0:T(8,128)(2,1)} %wk_ref.1, bf16[512,512]{1,0:T(8,128)(2,1)} %wv_ref.1, bf16[512,512]{1,0:T(8,128)(2,1)} %wq_ref.1, bf16[512,256]{1,0:T(8,128)(2,1)} %wp_ref.2, ...), custom_call_target="tpu_custom_call" | custom-call | flops 4000000000 | bytes 6000000 | tf_op jit(solution)/shard_map/gather_project/pallas_call | solution.py:340
  71.5 1.0 slice_bitcast_fusion.1
  72.5 0.1 fusion.4
  72.7 59.7 %stick_attention.1 = (bf16[16,64,256]{2,1,0:T(8,128)(2,1)}, bf16[512,2048]{1,0:T(8,128)(2,1)}, bf16[1024,2048]{1,0:T(8,128)(2,1)}, bf16[32,768]{1,0:T(8,128)(2,1)}) custom-call(f32[1,8]{1,0:T(1,128)} %bitcast.26, bf16[16,192,256]{2,1,0:T(8,128)(2,1)} %get-tuple-element.12.x_ref, bf16[256,512]{1,0:T(8,128)(2,1)} %wp_ref.3, bf16[512,512]{1,0:T(8,128)(2,1)} %wa_ref.1, ...), custom_call_target="tpu_custom_call" | custom-call | flops 40000000000 | bytes 4000000 | tf_op jit(solution)/shard_map/stick_attention/pallas_call | solution.py:656
  132.4 1.2 multiply_reduce_fusion
  133.6 0.7 slice_reduce_fusion.3
  134.3 0.7 slice_reduce_fusion.1
  135.1 1.2 fusion.3
  136.3 0.0 copy-start
  136.3 3.6 %fusion.11 = f32[256,2048]{1,0:T(8,128)S(1)} fusion(bf16[1024,256]{1,0:T(8,128)(2,1)S(1)} %fusion.3, bf16[1024,2048]{1,0:T(8,128)(2,1)} %get-tuple-element.16), kind=kOutput, calls=%fused_computation.26 | convolution fusion | flops 1073741824 | bytes 6815744 | tf_op jit(solution)/shard_map/dot_general | solution.py:730
  139.9 0.0 copy-done
  139.9 1.7 %fusion.1 = bf16[1,256,2048]{2,1,0:T(8,128)(2,1)} fusion(f32[256,2048]{1,0:T(8,128)S(1)} %fusion.11, bf16[512,2048]{1,0:T(8,128)(2,1)S(1)} %copy-done, f32[512]{0:T(512)S(1)} %maximum_convert_fusion.1, f32[256]{0:T(256)S(1)} %add_rsqrt_fusion.1, bf16[256,256]{1,0:T(8,128)(2,1)S(1)} %get-tuple-element.22, bf16[256,256]{1,0:T(8,128)(2,1)S(1)} %get-tuple-element.21), kind=kOutput, calls=%fused_computation.2 | convolution fusion | flops 538836992 | bytes 5508096 | tf_op jit(solution)/shard_map/dot_general | solution.py:730
  (4 shorter events, 0.0 us)
Async XLA Ops:
  136.3 3.6 %copy-start = (bf16[512,2048]{1,0:T(8,128)(2,1)S(1)}, bf16[512,2048]{1,0:T(8,128)(2,1)}, u32[]{:S(2)}) copy-start(bf16[512,2048]{1,0:T(8,128)(2,1)} %get-tuple-element.14) | copy-start | bytes 6291460

commit v5 on v4

v5 whole, which is shorter than its diff:
```python
import math

import jax
import jax.numpy as jnp
from jax import lax
from jax.experimental import pallas as pl
from jax.experimental.pallas import tpu as pltpu
from jax.sharding import PartitionSpec as P

HEADS = 16
HEAD_DIM = 64
POOL = 512
POOL_GROUPS = 4
BLOCKS = 16
HALF = 256
BLOCK = 512

EPS = 1e-06
LOG2E = 1.4426950408889634


def split_terms(value):
    high = value.astype(jnp.bfloat16)
    rest = value - high.astype(jnp.float32)
    middle = rest.astype(jnp.bfloat16)
    low = (rest - middle.astype(jnp.float32)).astype(jnp.bfloat16)
    return (high, middle, low)


MESH = pl.DeviceIdType.MESH


def mixer_kernel(
    tok_ref, gain_ref, wk_ref, wv_ref, wq_ref, wp_ref, kg_ref, qg_ref, mix_ref, scale_ref,
    offset_ref, wpo_ref, wao_ref, pg_ref, ag_ref,
    mixed_ref,
    buf, pbuf, tok_s, x_s, acc, acc_p, heads_s, pool_in, before_s, pooled_s, pool_rows,
    recv_s, other_s, o_ref, wp_all, wa_all, gains_m, gains_o, offset_m, offset_s,
    q_s, k_s, v_s, tri_s, mask_s, acc_s, carry_s, done_s,
    z0, z1, z2, l0, l1, l2, w0, w1, w2, send, recv,
):
    sp, y, core = lax.axis_index("sp"), lax.axis_index("fs"), lax.axis_index("tp")
    z, x = sp // 4, sp % 4
    y_up, y_down, y_far = (y + 1) % 4, (y + 3) % 4, (y + 2) % 4
    x_up, x_down, x_far = (x + 1) % 4, (x + 3) % 4, (x + 2) % 4
    z_up, z_down, z_far = (z + 1) % 4, (z + 3) % 4, (z + 2) % 4

    def at(z_to, x_to, y_to, core_to):
        return {"sp": z_to * 4 + x_to, "fs": y_to, "tp": core_to}

    partner = at(z, x, y, 1 - core)
    to = {
        "yp": at(z, x, y_up, core), "ym": at(z, x, y_down, core),
        "xp": at(z, x_up, y, core), "xm": at(z, x_down, y, core),
        "zp": at(z_up, x, y, core), "zm": at(z_down, x, y, core),
    }

    barrier = pltpu.get_barrier_semaphore()
    for target in (partner, to["yp"], to["ym"]):
        pl.semaphore_signal(barrier, inc=1, device_id=target, device_id_type=MESH)

    def greet(i, unused):
        for of_core in range(2):
            pl.semaphore_signal(
                barrier, inc=1, device_id={"sp": (sp + i) % BLOCKS, "fs": y, "tp": of_core},
                device_id_type=MESH,
            )
        return unused

    lax.fori_loop(1, BLOCKS, greet, 0)
    pl.semaphore_wait(barrier, 33)

    started = []

    def remote(source, target_ref, index, target):
        return pltpu.make_async_remote_copy(
            src_ref=source, dst_ref=target_ref, send_sem=send.at[index],
            recv_sem=recv.at[index], device_id=target, device_id_type=MESH,
        )

    def go(source, target_ref, index, target):
        copy = remote(source, target_ref, index, target)
        copy.start()
        started.append(copy)

    def got(target_ref, index):
        remote(target_ref, target_ref, index, partner).wait_recv()

    def rows(start, count=64):
        return pl.ds(pl.multiple_of(start, 32), count)

    weights = (wk_ref, wv_ref, wq_ref)
    quarters = (y_down, y_up, y_far)

    def part(a, quarter, start, count=64):
        return buf.at[a, quarter, rows(start, count), :]

    def direct(a):
        base = a * 30
        own_x, own_z = 64 * x, 256 + 64 * z
        w = weights[a]
        go(w.at[rows(own_x), :], part(a, y, own_x), base + 0, to["yp"])
        go(w.at[rows(own_z), :], part(a, y, own_z), base + 1, to["ym"])
        go(w.at[rows(own_x), :], part(a, y, own_x), base + 2, to["ym"])
        go(w.at[rows(own_z), :], part(a, y, own_z), base + 3, to["yp"])

    def ring_base(a, item, ring):
        return a * 30 + 6 + item * 8 + ring * 4

    own_row = (64 * x, 256 + 64 * z)
    down_row = (64 * x_down, 256 + 64 * z_down)
    up_row = (64 * x_up, 256 + 64 * z_up)
    far_row = (64 * x_far, 256 + 64 * z_far)
    ups = ("xp", "zp")
    downs = ("xm", "zm")

    def spread(a, item, ring):
        base = ring_base(a, item, ring)
        piece = part(a, quarters[item], own_row[ring])
        go(piece, piece, base + 0, to[ups[ring]])
        go(piece, piece, base + 1, to[downs[ring]])

    def relay(a, item, ring):
        base = ring_base(a, item, ring)
        q = quarters[item]
        got(part(a, q, down_row[ring]), base + 0)
        piece = part(a, q, down_row[ring], 32)
        go(piece, piece, base + 2, to[ups[ring]])
        got(part(a, q, up_row[ring]), base + 1)
        piece = part(a, q, up_row[ring] + 32, 32)
        go(piece, piece, base + 3, to[downs[ring]])

    def settle(a):
        for item in range(3):
            for ring in range(2):
                base = ring_base(a, item, ring)
                q = quarters[item]
                got(part(a, q, far_row[ring], 32), base + 2)
                got(part(a, q, far_row[ring] + 32, 32), base + 3)

    def first(a):
        base = a * 30
        piece = part(a, y_down, own_row[0])
        got(piece, base + 0)
        go(piece, piece, base + 4, to["yp"])
        spread(a, 0, 0)
        piece = part(a, y_up, own_row[1])
        got(piece, base + 1)
        go(piece, piece, base + 5, to["ym"])
        spread(a, 1, 1)
        got(part(a, y_up, own_row[0]), base + 2)
        spread(a, 1, 0)
        got(part(a, y_down, own_row[1]), base + 3)
        spread(a, 0, 1)

    def second(a):
        relay(a, 0, 0)
        relay(a, 1, 1)

    def third(a):
        base = a * 30
        got(part(a, y_far, own_row[0]), base + 4)
        spread(a, 2, 0)
        got(part(a, y_far, own_row[1]), base + 5)
        spread(a, 2, 1)
        relay(a, 1, 0)
        relay(a, 0, 1)

    def fourth(a):
        relay(a, 2, 0)
        relay(a, 2, 1)

    def query_direct():
        go(wq_ref, buf.at[2, y], 60, to["yp"])
        go(wq_ref, buf.at[2, y], 61, to["ym"])

    def query_relay():
        got(buf.at[2, y_down], 60)
        piece = buf.at[2, y_down, 0:256, :]
        go(piece, piece, 62, to["yp"])
        got(buf.at[2, y_up], 61)
        piece = buf.at[2, y_up, 256:512, :]
        go(piece, piece, 63, to["ym"])

    def query_settle():
        got(buf.at[2, y_far, 0:256, :], 62)
        got(buf.at[2, y_far, 256:512, :], 63)

    pool_base = 90

    def pool_direct():
        go(wp_ref, pbuf.at[y], pool_base + 0, to["yp"])
        go(wp_ref, pbuf.at[y], pool_base + 1, to["ym"])

    def pool_relay():
        got(pbuf.at[y_down], pool_base + 0)
        piece = pbuf.at[y_down, 0:256, :]
        go(piece, piece, pool_base + 2, to["yp"])
        got(pbuf.at[y_up], pool_base + 1)
        piece = pbuf.at[y_up, 256:512, :]
        go(piece, piece, pool_base + 3, to["ym"])

    def pool_settle():
        got(pbuf.at[y_far, 0:256, :], pool_base + 2)
        got(pbuf.at[y_far, 256:512, :], pool_base + 3)

    def own(a):
        acc[a] = jnp.dot(x_s[y], weights[a][...], preferred_element_type=jnp.float32)

    def rest(a):
        total = acc[a]
        for q in quarters:
            total = total + jnp.dot(x_s[q], buf[a, q], preferred_element_type=jnp.float32)
        return total

    def head_copy(a, i, source):
        h, of_core = (sp + i // 2) % 8, i % 2
        return pltpu.make_async_remote_copy(
            src_ref=heads_s.at[a, h, of_core],
            dst_ref=recv_s.at[source, a * 64 : a * 64 + 64, :],
            send_sem=send.at[97 + a * 16 + i], recv_sem=recv.at[97 + a * 16 + source],
            device_id={"sp": 8 * core + h, "fs": y, "tp": of_core}, device_id_type=MESH,
        )

    stays = sp // 8 == core

    def deliver(a, total):
        turned = total.T.reshape(8, HEAD_DIM, BLOCK)
        if a != 1:
            factor = lax.rsqrt(jnp.mean(turned * turned, axis=1, keepdims=True) + EPS)
            gain_row = (kg_ref if a == 0 else qg_ref)[...]
            gain = jnp.broadcast_to(gain_row, (HEAD_DIM, HEAD_DIM)).T[:, 0:1]
            turned = turned * factor * gain[None]
        turned = turned.astype(jnp.bfloat16)
        heads_s[a, :, 0] = turned[:, :, :HALF]
        heads_s[a, :, 1] = turned[:, :, HALF:]

        def send_head(i, unused):
            @pl.when(jnp.logical_not(stays & (i == core)))
            def _():
                head_copy(a, i, sp).start()

            return unused

        lax.fori_loop(0, 16, send_head, 0)

        @pl.when(stays)
        def _():
            recv_s[sp, a * 64 : a * 64 + 64, :] = heads_s[a, sp % 8, core]

    def wa_part(quarter, of_core, start, count):
        return wa_all.at[
            pl.ds(pl.multiple_of(of_core * 512 + start, 128), count),
            pl.ds(pl.multiple_of(quarter * 512, 512), 512),
        ]

    def wp_part(quarter, of_core, start, count):
        return wp_all.at[
            pl.ds(pl.multiple_of(of_core * 256 + start, 128), count),
            pl.ds(pl.multiple_of(quarter * 512, 512), 512),
        ]

    def share(quarter, index):
        go(wa_part(quarter, core, 0, 512), wa_part(quarter, core, 0, 512), index, partner)
        go(wp_part(quarter, core, 0, 256), wp_part(quarter, core, 0, 256), index + 1, partner)

    def shared(quarter, index):
        got(wa_part(quarter, 1 - core, 0, 512), index)
        got(wp_part(quarter, 1 - core, 0, 256), index + 1)

    def weights_start():
        go(wao_ref, wa_part(y, core, 0, 512), 147, to["yp"])
        go(wpo_ref, wp_part(y, core, 0, 256), 148, to["yp"])
        go(wao_ref, wa_part(y, core, 0, 512), 149, to["ym"])
        go(wpo_ref, wp_part(y, core, 0, 256), 150, to["ym"])
        go(wao_ref, wa_part(y, core, 0, 512), 155, partner)
        go(wpo_ref, wp_part(y, core, 0, 256), 156, partner)

    def weights_middle():
        got(wa_part(y_down, core, 0, 512), 147)
        got(wp_part(y_down, core, 0, 256), 148)
        go(wa_part(y_down, core, 0, 256), wa_part(y_down, core, 0, 256), 151, to["yp"])
        go(wp_part(y_down, core, 0, 128), wp_part(y_down, core, 0, 128), 152, to["yp"])
        got(wa_part(y_up, core, 0, 512), 149)
        got(wp_part(y_up, core, 0, 256), 150)
        go(wa_part(y_up, core, 256, 256), wa_part(y_up, core, 256, 256), 153, to["ym"])
        go(wp_part(y_up, core, 128, 128), wp_part(y_up, core, 128, 128), 154, to["ym"])
        share(y_down, 157)
        share(y_up, 159)

    def weights_late():
        got(wa_part(y_far, core, 0, 256), 151)
        got(wp_part(y_far, core, 0, 128), 152)
        got(wa_part(y_far, core, 256, 256), 153)
        got(wp_part(y_far, core, 128, 128), 154)
        share(y_far, 161)

    def weights_end():
        shared(y, 155)
        shared(y_down, 157)
        shared(y_up, 159)
        shared(y_far, 161)

    mine_at = pl.ds(pl.multiple_of(core * HALF, HALF), HALF)
    other_at = pl.ds(pl.multiple_of((1 - core) * HALF, HALF), HALF)

    def turned(block):
        return block.astype(jnp.float32).T.astype(jnp.bfloat16)

    def forward(a, r):
        return pltpu.make_async_remote_copy(
            src_ref=recv_s.at[r, a * 64 : a * 64 + 64, :],
            dst_ref=other_s.at[r, a * 64 : a * 64 + 64, :],
            send_sem=send.at[200 + a * 16 + r], recv_sem=recv.at[200 + a * 16 + r],
            device_id=partner, device_id_type=MESH,
        )

    def place(a, r, block, at):
        if a == 0:
            k_s[r, at, 0:64] = turned(block)
        elif a == 1:
            v_s[r, :, at] = block
        else:
            q_s[r, 0:64, :] = block

    def take(a):
        def pair(n, unused):
            places_now = [(sp + 2 * n) % BLOCKS, (sp + 2 * n + 1) % BLOCKS]
            for r in places_now:
                @pl.when(jnp.logical_not(stays & (r == sp)))
                def _():
                    head_copy(a, 0, r).wait_recv()

                if a < 2:
                    forward(a, r).start()
            for r in places_now:
                place(a, r, recv_s[r, a * 64 : a * 64 + 64, :], mine_at)
            return unused

        lax.fori_loop(0, BLOCKS // 2, pair, 0)

    def take_other(a):
        def pair(n, unused):
            places_now = [(sp + 2 * n) % BLOCKS, (sp + 2 * n + 1) % BLOCKS]
            for r in places_now:
                forward(a, r).wait_recv()
            for r in places_now:
                place(a, r, other_s[r, a * 64 : a * 64 + 64, :], other_at)
            return unused

        lax.fori_loop(0, BLOCKS // 2, pair, 0)

    scale = LOG2E / math.sqrt(HEAD_DIM)
    half = core
    go(tok_ref, tok_s, 94, partner)
    direct(0)
    direct(1)
    offset_m[...] = jnp.zeros_like(offset_m)
    offset_m[:, 0:8] = jnp.broadcast_to(offset_ref[...], (8, 8))
    gains_m[:, 0:256] = jnp.broadcast_to(pg_ref[...], (16, 256))
    gains_m[:, 256:768] = jnp.broadcast_to(ag_ref[...], (16, 512))
    tri_s[...] = jnp.where(
        lax.broadcasted_iota(jnp.int32, (HALF, HALF), 0)
        <= lax.broadcasted_iota(jnp.int32, (HALF, HALF), 1),
        1.0,
        0.0,
    ).astype(jnp.bfloat16)
    go(offset_m, offset_s, 163, partner)
    go(gains_m, gains_o, 146, partner)
    got(tok_s, 94)

    mine_f = tok_ref[...].astype(jnp.float32)
    other_f = tok_s[...].astype(jnp.float32)
    squares = jnp.sum(mine_f * mine_f, axis=1, keepdims=True) + jnp.sum(
        other_f * other_f, axis=1, keepdims=True
    )
    factor = lax.rsqrt(squares / 2048.0 + EPS)
    for j in range(2):
        columns = slice(512 * j, 512 * j + 512)
        at_mine = 2 * core + j
        at_other = 2 * (1 - core) + j
        x_s[at_mine] = (
            tok_ref[:, columns].astype(jnp.float32) * factor * gain_ref[at_mine]
        ).astype(jnp.bfloat16)
        x_s[at_other] = (
            tok_s[:, columns].astype(jnp.float32) * factor * gain_ref[at_other]
        ).astype(jnp.bfloat16)

    first(0)
    own(0)
    own(1)
    first(1)
    query_direct()
    own(2)
    second(0)
    acc_p[...] = jnp.dot(x_s[y], wp_ref[...], preferred_element_type=jnp.float32)
    third(0)
    second(1)
    fourth(0)
    third(1)
    settle(0)
    deliver(0, rest(0))
    fourth(1)
    settle(1)
    deliver(1, rest(1))
    query_relay()
    pool_direct()
    got(offset_s, 163)
    of_core = jnp.where(sp // 8 == core, offset_m[0:1, :], offset_s[0:1, :])
    chosen = lax.broadcasted_iota(jnp.int32, (1, 128), 1) == sp % 8
    offset = jnp.sum(jnp.where(chosen, of_core, 0.0), axis=1, keepdims=True) * math.sqrt(HEAD_DIM)
    column = lax.broadcasted_iota(jnp.int32, (BLOCK, 64), 1)
    terms = split_terms(jnp.broadcast_to(offset, (BLOCK, 64)))
    extra = jnp.where(
        column == 0,
        terms[0].astype(jnp.float32),
        jnp.where(
            column == 1,
            terms[1].astype(jnp.float32),
            jnp.where(column == 2, terms[2].astype(jnp.float32), 0.0),
        ),
    ).astype(jnp.bfloat16)
    row = lax.broadcasted_iota(jnp.int32, (64, HALF), 0)
    ones = jnp.where(row < 3, 1.0, 0.0).astype(jnp.bfloat16)
    mask_s[...] = jnp.where(
        lax.broadcasted_iota(jnp.int32, (BLOCK, HALF), 0)
        < lax.broadcasted_iota(jnp.int32, (BLOCK, HALF), 1) + half * HALF,
        0.0,
        -1e30,
    )
    acc_s[...] = jnp.zeros_like(acc_s)
    carry_s[...] = jnp.zeros_like(carry_s)


    def fill(r, unused):
        k_s[r, :, 64:128] = extra
        q_s[r, 64:128, :] = ones
        return unused

    lax.fori_loop(0, BLOCKS, fill, 0)
    mine_half = pl.ds(pl.multiple_of(core * HALF, HALF), HALF)
    other_half = pl.ds(pl.multiple_of((1 - core) * HALF, HALF), HALF)
    take(0)
    query_settle()
    deliver(2, rest(2))
    pool_relay()
    weights_start()
    take(1)
    take_other(0)
    wa_part(y, core, 0, 512)[...] = wao_ref[...]
    wp_part(y, core, 0, 256)[...] = wpo_ref[...]
    pool_settle()
    total = acc_p[...]
    for q in quarters:
        total = total + jnp.dot(x_s[q], pbuf[q], preferred_element_type=jnp.float32)
    pool_in[...] = total.astype(jnp.bfloat16)
    tail = pool_in.at[BLOCK - 16 : BLOCK, :]
    go(tail, before_s, 95, {"sp": (sp + 1) % BLOCKS, "fs": y, "tp": core})
    current = pool_in[...].astype(jnp.float32)
    got(before_s, 95)
    before = jnp.where(sp == 0, 0.0, before_s[...].astype(jnp.float32))

    def behind(values, count):
        return jnp.concatenate([jnp.zeros((count, values.shape[1]), jnp.float32), values[:-count]], axis=0)

    extended = jnp.concatenate([before, current], axis=0)
    sum_2 = extended + behind(extended, 1)
    sum_4 = sum_2 + behind(sum_2, 2)
    sum_8 = sum_4 + behind(sum_4, 4)
    sum_16 = sum_8 + behind(sum_8, 8)
    position = lax.broadcasted_iota(jnp.int32, (BLOCK, 128), 0) + (sp * BLOCK + 1)
    for group in range(2):
        columns = slice(128 * group, 128 * group + 128)
        low, high = ((sum_2, sum_8), (sum_4, sum_16))[group]
        window = jnp.where(core == 0, 2 << group, 8 << group)
        summed = jnp.where(core == 0, low[16:, columns], high[16:, columns])
        counted = jnp.minimum(position, window).astype(jnp.float32)
        centered = (summed / counted - current[:, columns]).astype(jnp.bfloat16)
        mixed = jnp.dot(centered, mix_ref[group], preferred_element_type=jnp.float32)
        pooled_s[:, columns] = (mixed * scale_ref[:, columns]).astype(jnp.bfloat16)
    mine_rows = pl.ds(pl.multiple_of(core * HALF, HALF), HALF)
    other_rows = pl.ds(pl.multiple_of((1 - core) * HALF, HALF), HALF)
    go(pooled_s.at[other_rows, :], pool_rows.at[core], 96, partner)
    pool_rows[core] = pooled_s[mine_rows, :]
    take_other(1)
    take(2)

    zs, ls, ws = (z0, z1, z2), (l0, l1, l2), (w0, w1, w2)

    first_row = jnp.where(sp == BLOCKS - 1, 1, sp + 1)

    def places(state):
        step, r, distance = state
        row_at = jnp.where((step < 0) | (step >= 136), BLOCKS, r)
        return (row_at, r, jnp.maximum(r - distance, 0))

    def advance(state):
        step, r, distance = state
        diagonal = step < BLOCKS - 1
        turn = step == BLOCKS - 1
        done = distance >= r
        next_row = jnp.where(r == BLOCKS - 1, 1, r + 1)
        r_after = jnp.where(
            diagonal,
            jnp.maximum(step + 1, 0),
            jnp.where(turn, first_row, jnp.where(done, next_row, r)),
        )
        after = jnp.where(diagonal, 0, jnp.where(turn | done, 1, distance + 1))
        return (step + 1, r_after, after)

    def scores(state, b, masked):
        unused_row, r, g = places(state)
        z = jnp.dot(k_s[g], q_s[r], preferred_element_type=jnp.float32) * scale
        if masked:
            z = z + mask_s[...]
        zs[b][...] = z

    def soften(b):
        ls[b][...] = jnp.log2(1.0 + jnp.exp2(zs[b][...])).astype(jnp.bfloat16)

    def weigh(state, b):
        row_at = places(state)[0]
        late = jnp.dot(tri_s[...], ls[b][HALF:, :], preferred_element_type=jnp.float32)
        early = jnp.dot(tri_s[...], ls[b][:HALF, :], preferred_element_type=jnp.float32)
        carry = carry_s[row_at][0:1]
        before = carry + late[0:1]
        ws[b][HALF:, :] = jnp.exp2(zs[b][HALF:, :] - (late + carry)).astype(jnp.bfloat16)
        ws[b][:HALF, :] = jnp.exp2(zs[b][:HALF, :] - (early + before)).astype(jnp.bfloat16)
        carry_s[row_at] = jnp.broadcast_to(before + early[0:1], (8, HALF))

    def gather_values(state, b):
        row_at, unused_row, g = places(state)
        acc_s[row_at] = acc_s[row_at] + jnp.dot(
            v_s[g], ws[b][...], preferred_element_type=jnp.float32
        )

    def return_row(state):
        step, r, distance = state

        @pl.when((distance == r) & (step >= 0) & (step < 136))
        def _():
            done_s[r] = acc_s[r].astype(jnp.bfloat16)

            @pl.when(r != sp)
            def _():
                pltpu.make_async_remote_copy(
                    src_ref=done_s.at[r], dst_ref=o_ref.at[sp], send_sem=send.at[180 + r],
                    recv_sem=recv.at[180 + sp], device_id={"sp": r, "fs": y, "tp": core}, device_id_type=MESH,
                ).start()

    def steps(masked):
        def body(n, states):
            states = list(states)
            for unused_step in range(6):
                states.append(advance(states[-1]))
            for u in range(6):
                gather_values(states[u], (u + 2) % 3)
                weigh(states[u + 1], u % 3)
                soften((u + 1) % 3)
                scores(states[u + 3], (u + 2) % 3, masked)
            for u in range(6):
                return_row(states[u])
            return tuple(states[6:])

        return body

    first_states = tuple(
        (jnp.int32(step), jnp.int32(0), jnp.int32(0)) for step in (-5, -4, -3, -2)
    )
    states = lax.fori_loop(0, 3, steps(True), first_states)
    states = lax.fori_loop(0, 8, steps(False), states)
    weights_middle()
    states = lax.fori_loop(8, 14, steps(False), states)
    weights_late()
    lax.fori_loop(14, 21, steps(False), states)
    o_ref[sp] = done_s[sp]
    weights_end()
    got(gains_o, 146)
    got(pool_rows.at[1 - core], 96)

    def settle_row(i, unused):
        r = (sp + i) % BLOCKS
        copy = pltpu.make_async_remote_copy(
            src_ref=done_s.at[r], dst_ref=o_ref.at[r], send_sem=send.at[180 + r],
            recv_sem=recv.at[180 + r], device_id={"sp": r, "fs": y, "tp": core},
            device_id_type=MESH,
        )
        copy.wait_send()
        copy.wait_recv()
        return unused

    lax.fori_loop(1, BLOCKS, settle_row, 0)

    def gain_rows(columns):
        mine_gain = gains_m[0:1, columns].astype(jnp.float32)
        other_gain = gains_o[0:1, columns].astype(jnp.float32)
        low = jnp.where(core == 0, mine_gain, other_gain)
        high = jnp.where(core == 0, other_gain, mine_gain)
        return jnp.concatenate([low, high], axis=1)

    attended = o_ref[...].reshape(HEADS * HEAD_DIM, HALF).astype(jnp.float32).T
    factor = lax.rsqrt(jnp.mean(attended * attended, axis=1, keepdims=True) + EPS)
    attn_normed = (attended * factor * gain_rows(slice(256, 768))).astype(jnp.bfloat16)
    pooled = jnp.concatenate([pool_rows[0], pool_rows[1]], axis=1).astype(jnp.float32)
    factor = lax.rsqrt(jnp.mean(pooled * pooled, axis=1, keepdims=True) + EPS)
    pool_normed = (pooled * factor * gain_rows(slice(0, 256))).astype(jnp.bfloat16)
    for j in range(4):
        columns = slice(512 * j, 512 * j + 512)
        mixed_ref[:, columns] = (
            jnp.dot(pool_normed, wp_all[:, columns], preferred_element_type=jnp.float32)
            + jnp.dot(attn_normed, wa_all[:, columns], preferred_element_type=jnp.float32)
        ).astype(jnp.bfloat16)

    for copy in started:
        copy.wait_send()

    def settle_heads(i, unused):
        for a in range(3):
            @pl.when(jnp.logical_not(stays & (i == core)))
            def _():
                head_copy(a, i, sp).wait_send()

        for a in range(2):
            forward(a, i).wait_send()
        return unused

    lax.fori_loop(0, BLOCKS, settle_heads, 0)


def mixer(*operands):
    vmem = pl.BlockSpec(memory_space=pltpu.VMEM)
    return pl.pallas_call(
        mixer_kernel,
        out_shape=jax.ShapeDtypeStruct((HALF, 2048), jnp.bfloat16),
        in_specs=[vmem] * 15,
        out_specs=vmem,
        scratch_shapes=[
            pltpu.VMEM((3, 4, 512, 512), jnp.bfloat16),
            pltpu.VMEM((4, 512, 256), jnp.bfloat16),
            pltpu.VMEM((512, 1024), jnp.bfloat16),
            pltpu.VMEM((4, 512, 512), jnp.bfloat16),
            pltpu.VMEM((3, 512, 512), jnp.float32),
            pltpu.VMEM((512, 256), jnp.float32),
            pltpu.VMEM((3, 8, 2, HEAD_DIM, HALF), jnp.bfloat16),
            pltpu.VMEM((512, 256), jnp.bfloat16),
            pltpu.VMEM((16, 256), jnp.bfloat16),
            pltpu.VMEM((512, 256), jnp.bfloat16),
            pltpu.VMEM((2, HALF, 256), jnp.bfloat16),
            pltpu.VMEM((BLOCKS, 3 * HEAD_DIM, HALF), jnp.bfloat16),
            pltpu.VMEM((BLOCKS, 2 * HEAD_DIM, HALF), jnp.bfloat16),
            pltpu.VMEM((BLOCKS, HEAD_DIM, HALF), jnp.bfloat16),
            pltpu.VMEM((512, 2048), jnp.bfloat16),
            pltpu.VMEM((1024, 2048), jnp.bfloat16),
            pltpu.VMEM((16, 768), jnp.bfloat16),
            pltpu.VMEM((16, 768), jnp.bfloat16),
            pltpu.VMEM((8, 128), jnp.float32),
            pltpu.VMEM((8, 128), jnp.float32),
            pltpu.VMEM((BLOCKS, 128, HALF), jnp.bfloat16),
            pltpu.VMEM((BLOCKS, BLOCK, 128), jnp.bfloat16),
            pltpu.VMEM((BLOCKS, HEAD_DIM, BLOCK), jnp.bfloat16),
            pltpu.VMEM((HALF, HALF), jnp.bfloat16),
            pltpu.VMEM((BLOCK, HALF), jnp.float32),
            pltpu.VMEM((BLOCKS + 1, HEAD_DIM, HALF), jnp.float32),
            pltpu.VMEM((BLOCKS + 1, 8, HALF), jnp.float32),
            pltpu.VMEM((BLOCKS, HEAD_DIM, HALF), jnp.bfloat16),
            *[pltpu.VMEM((BLOCK, HALF), jnp.float32)] * 3,
            *[pltpu.VMEM((BLOCK, HALF), jnp.bfloat16)] * 6,
            pltpu.SemaphoreType.DMA((232,)),
            pltpu.SemaphoreType.DMA((232,)),
        ],
        compiler_params=pltpu.CompilerParams(
            collective_id=0, has_side_effects=True, vmem_limit_bytes=62 * 1024 * 1024
        ),
        cost_estimate=pl.CostEstimate(
            flops=45_000_000_000, bytes_accessed=8_000_000, transcendentals=50_000_000
        ),
        name="token_mixer",
    )(*operands)


def shards(
    tokens,
    norm_gain,
    w_pool_in,
    w_query,
    w_key,
    w_value,
    query_gain,
    key_gain,
    stick_offset,
    pool_mix,
    pool_scale,
    pool_gain,
    attn_gain,
    w_out_pool,
    w_out_attn,
):
    mixed = mixer(
        tokens[0], norm_gain.reshape(4, 1, 512), w_key, w_value, w_query, w_pool_in,
        key_gain.reshape(1, HEAD_DIM), query_gain.reshape(1, HEAD_DIM), pool_mix,
        pool_scale.reshape(1, 256), stick_offset.reshape(1, 8), w_out_pool, w_out_attn,
        pool_gain.reshape(1, 256), attn_gain.reshape(1, 512),
    )
    return mixed[None]


def solution(mesh):
    in_specs = (
        P("fs", "sp", "tp"),
        P(),
        P("fs", "tp"),
        P("fs", "tp"),
        P("fs", "tp"),
        P("fs", "tp"),
        P(),
        P(),
        P("tp"),
        P("tp", None, None),
        P("tp"),
        P("tp"),
        P("tp"),
        P("tp", "fs"),
        P("tp", "fs"),
    )
    out_specs = P("fs", ("sp", "tp"), None)
    return jax.shard_map(shards, mesh=mesh, in_specs=in_specs, out_specs=out_specs, check_vma=False)
```

time: 143 us -> 123 us (0.86)
  the two profiles are of different devices: /device:TPU:1 before, /device:TPU:2 now
where the time goes in v5:
time: 123 us
  Pallas kernels  119 us (97%)
  local copies, waits for them, and re-layouts  4.22 us (3%)
    pallas_call x1, Pallas kernels, mixer(): pl.pallas_call(mixer_kernel, out_shape=jax.ShapeDtypeStruct((HALF, 2048),...  119 us
    unnamed x5, local copies, waits for them, and re-layouts  3.07 us

profile of v5, /device:TPU:2, one launch (start us, length us, event | category | flops | bytes accessed | tf_op | source)
XLA Modules:
  0.0 122.9 jit_solution(8210131017050743973)
XLA Ops:
  0.0 0.0 copy-start.1
  0.0 0.7 copy-done.1
  0.7 0.0 copy-start
  0.7 0.6 reshape.26.pg_ref
  1.2 0.1 copy-done
  1.3 0.6 reshape.27.ag_ref
  1.9 118.7 %token_mixer.1 = bf16[256,2048]{1,0:T(8,128)(2,1)} custom-call(bf16[512,1024]{1,0:T(8,128)(2,1)} %bitcast.8, f32[4,1,512]{2,1,0:T(1,128)} %bitcast.9, bf16[512,512]{1,0:T(8,128)(2,1)} %wk_ref.1, bf16[512,512]{1,0:T(8,128)(2,1)} %wv_ref.1, bf16[512,512]{1,0:T(8,128)(2,1)} %wq_ref.1, bf16[512,256]{1,0:T(8,128)(2,1)} %wp_ref.1, f32[1,64]{1,0:T(1,128)} %bitcast.11, ...), custom_call_target="tpu_custom_call" | custom-call | flops 44999999488 | bytes 8000000 | tf_op jit(solution)/shard_map/token_mixer/pallas_call | solution.py:632
  120.6 2.3 %copy.17 = bf16[1,256,2048]{2,1,0:T(8,128)(2,1)} copy(bf16[1,256,2048]{2,1,0:T(8,128)(2,1)} %bitcast.7) | data formatting | bytes 2097152
Async XLA Ops:
  0.0 0.7 copy-start.1
  0.7 0.7 copy-start
